TPU v7x, 256 devices: a 4x2x16 block of a 4x16x16 slice. The times are simulated.
256 devices in a mesh: grp: 2 (over y), sp: 32 (over z, core), tp: 4 (over x).
Axes of the slice: x: 4, y: 2, z: 16, core: 2. Of those that a mesh axis runs over, the one named last changes fastest.
The devices are a block of a 4x16x16 slice.
Arguments:
- query_plain: bfloat16 [10240, 1024], P(('grp', 'sp'), 'tp'), parts along dimension 0, may hold values from -6 to 6
- query_turn: bfloat16 [10240, 512], P(('grp', 'sp'), 'tp'), parts along dimension 0, may hold values from -40 to 40, as said below
- latent: bfloat16 [10240, 512], P(('grp', 'sp')), parts along dimension 0, may hold values from -6 to 6
- key_turn: bfloat16 [10240, 64], P(('grp', 'sp')), parts along dimension 0, may hold values from -40 to 40, as said below
- latent_norm_scale: bfloat16 [512], replicated, may hold values from 0.099609375 to 1.8984375
- plain_key_matrix: bfloat16 [512, 1024], P(None, 'tp'), may hold values from -0.25 to 0.25
- value_matrix: bfloat16 [512, 1024], P(None, 'tp'), may hold values from -0.25 to 0.25
- residual: bfloat16 [10240, 2048], P(('grp', 'sp', 'tp')), parts along dimension 0, may hold values from -6 to 6
- out_weight: bfloat16 [1024, 2048], replicated, may hold values from -6 to 6
- ffn_gain: bfloat16 [2048], replicated, may hold values from 0.099609375 to 1.8984375
- gate_weight: bfloat16 [32, 2048, 1024], P('sp', None, 'tp'), may hold values from -1 to 1
- up_weight: bfloat16 [32, 2048, 1024], P('sp', None, 'tp'), may hold values from -1 to 1
- down_weight: bfloat16 [32, 1024, 2048], P('sp', 'tp'), may hold values from -0.0625 to 0.0625
- routes: int32 [10240, 4], P(('grp', 'sp', 'tp')), parts along dimension 0, may hold values from 0 to 31, all different within a row; in each aligned block of 40 rows (0 to 39, 40 to 79, ...) at most 7 rows name the same one
- route_weights: float32 [10240, 4], P(('grp', 'sp', 'tp')), parts along dimension 0, may hold values from 0.1 to 0.6
Outputs:
- mixed: bfloat16 [10240, 2048], P(('grp', 'sp', 'tp')), parts along dimension 0
There are 2 independent parts, one for each index of `grp`. A program takes and returns all parts, laid end to end along the dimension named above; an argument that names none is the same for every part. Nothing has to cross between parts.
Inputs may be any that keep to these rules, and one draw needn't show every extreme that they name: `query_turn`: in the hidden draw some rows are large. `key_turn`: in the hidden draw some rows are large. `routes`: each row names 4 different experts. In each aligned block of 40 rows (the rows of one device) no expert is named more than 7 times, a bound that some block reaches.
All inputs are finite; a program needn't handle non-finite values.
Results may differ from a plain program's by a relative error of at most 0.015.
Values may be sent and summed in bfloat16 or wider, within the bound.
A program may use at most 128 MiB of HBM per device.

v0:
```python
import jax
import jax.numpy as jnp
from jax import lax
from jax.sharding import Mesh
from jax.sharding import PartitionSpec as P

PLAIN_HEAD_WIDTH = 128
QK_ROPE = 64
VALUE_WIDTH = 128
GRID_W = 64
SP = ("sp_0", "sp_1")
GRP_SP = ("grp", "sp_0", "sp_1")
GRP_SP_TP = ("grp", "sp_0", "sp_1", "tp")


theta = 10000.0
eps = 1e-06
limit = 7.0
slope = 1.702


def sent_together(arrays, axis, dim, along):
    both = jnp.concatenate(arrays, axis=along)
    result, at, finished = (lax.all_gather(both, axis, axis=dim, tiled=True), 0, [])
    for a in arrays:
        finished.append(lax.slice_in_dim(result, at, at + a.shape[along], axis=along))
        at += a.shape[along]
    return tuple(finished)


def turned_gather(arrays, axis, dims):
    turned = [jnp.moveaxis(a, dim, 0) for a, dim in zip(arrays, dims)]
    both = jnp.concatenate([t.reshape(len(t), -1) for t in turned], axis=1)
    result, at, finished = (lax.all_gather(both, axis, axis=0, tiled=True), 0, [])
    for t, dim in zip(turned, dims):
        share = result[:, at : at + t[0].size].reshape(-1, *t.shape[1:])
        finished.append(jnp.moveaxis(share, 0, dim))
        at += t[0].size
    return tuple(finished)


def cut_along(array, dim, count):
    lengths = array.shape
    blocks = array.reshape(*lengths[:dim], count, lengths[dim] // count, *lengths[dim + 1 :])
    return jnp.moveaxis(blocks, dim, 0)


def laid_out(blocks, dim):
    lengths = list(blocks.shape[1:])
    lengths[dim] *= blocks.shape[0]
    return jnp.moveaxis(blocks, 0, dim).reshape(lengths)


def moved_by_axis(blocks, axes, order):
    inside = blocks.shape[1:]
    result = blocks.reshape(*(lax.axis_size(a) for a in axes), *inside)
    for k in order:
        result = lax.all_to_all(result, axes[k], k, k, tiled=True)
    return result.reshape(-1, *inside)


def exchange_by_chip(array, groups, order, split_dim, concat_dim):
    count = lax.axis_size(groups[0]) * lax.axis_size(groups[1])
    blocks = cut_along(array, split_dim, count)
    return laid_out(moved_by_axis(blocks, groups, order), concat_dim)


def turn(vector, row_shift, col_shift):
    width = vector.shape[-1]
    count = width // 4
    half = width // 2
    freqs = theta ** (-jnp.arange(count, dtype=jnp.float32) / count)
    extra = (1,) * (vector.ndim - 2)
    pieces = []
    for portion, shift in ((vector[..., :half], row_shift), (vector[..., half:], col_shift)):
        angle = (shift.astype(jnp.float32)[:, None] * freqs[None, :]).reshape(
            (shift.shape[0],) + extra + (count,)
        )
        lower = portion[..., :count]
        upper = portion[..., count:]
        pieces.append(
            jnp.concatenate(
                [
                    lower * jnp.cos(angle) - upper * jnp.sin(angle),
                    lower * jnp.sin(angle) + upper * jnp.cos(angle),
                ],
                axis=-1,
            )
        )
    return jnp.concatenate(pieces, axis=-1)


def norm_scale(values, gain):
    wide = values.astype(jnp.float32)
    return (
        wide
        * lax.rsqrt(jnp.mean(wide * wide, axis=-1, keepdims=True) + eps)
        * gain.astype(jnp.float32)
    )


def expert_active(rows, gate_w, up_w):
    gate_pre = jnp.minimum(jnp.dot(rows, gate_w, preferred_element_type=jnp.float32), limit)
    up_pre = jnp.clip(jnp.dot(rows, up_w, preferred_element_type=jnp.float32), -limit, limit)
    return ((up_pre + 1.0) * gate_pre * jax.nn.sigmoid(slope * gate_pre)).astype(jnp.bfloat16)


def expert_whole(rows, gate_w, up_w, down_w, groups):
    active = expert_active(rows, gate_w, up_w)
    piece = down_w.shape[0] // groups
    total = jnp.zeros((rows.shape[0], down_w.shape[1]), jnp.float32)
    for index in range(groups):
        product = jnp.dot(
            active[:, index * piece : (index + 1) * piece],
            down_w[index * piece : (index + 1) * piece],
            preferred_element_type=jnp.float32,
        )
        total = total + product.astype(jnp.bfloat16).astype(jnp.float32)
    return total.astype(jnp.bfloat16)


def on_device(
    query_plain,
    query_turn,
    latent,
    key_turn,
    latent_norm_scale,
    plain_key_matrix,
    value_matrix,
    residual,
    out_weight,
    ffn_gain,
    gate_weight,
    up_weight,
    down_weight,
    routes,
    route_weights,
):
    tok_dev = latent.shape[0]
    heads_dev = query_plain.shape[1] // PLAIN_HEAD_WIDTH
    model_width = residual.shape[1]
    place = lax.axis_index(SP) * tok_dev + jnp.arange(tok_dev, dtype=jnp.int32)
    grid_row = place // GRID_W
    grid_col = place % GRID_W
    normed_latent = norm_scale(latent, latent_norm_scale).astype(jnp.bfloat16)
    key_plain = jnp.dot(normed_latent, plain_key_matrix, preferred_element_type=jnp.float32).astype(
        jnp.bfloat16
    )
    values = jnp.dot(normed_latent, value_matrix, preferred_element_type=jnp.float32).astype(
        jnp.bfloat16
    )
    key_rot = turn(key_turn.astype(jnp.float32), grid_row, grid_col).astype(jnp.bfloat16)
    key_pairs = key_rot.reshape(tok_dev // 2, 2 * QK_ROPE)
    query_rot = turn(
        query_turn.astype(jnp.float32).reshape(tok_dev, heads_dev, QK_ROPE), grid_row, grid_col
    ).astype(jnp.bfloat16)
    plain_query = query_plain.reshape(tok_dev, heads_dev, PLAIN_HEAD_WIDTH)
    scale = (PLAIN_HEAD_WIDTH + QK_ROPE) ** (-0.5)
    most = jnp.full((heads_dev, tok_dev), -jnp.inf, jnp.float32)
    total = jnp.zeros((heads_dev, tok_dev), jnp.float32)
    summed = jnp.zeros((heads_dev, tok_dev, VALUE_WIDTH), jnp.float32)
    piece_keys, piece_values, piece_pairs = (
        *sent_together((key_plain, values), SP, 0, 1),
        lax.all_gather(key_pairs, SP, axis=0, tiled=True),
    )
    count = piece_keys.shape[0]
    piece_rot = piece_pairs.reshape(count, QK_ROPE)
    new_most = []
    new_total = []
    new_summed = []
    for head in range(heads_dev):
        head_keys = piece_keys[:, head * PLAIN_HEAD_WIDTH : (head + 1) * PLAIN_HEAD_WIDTH]
        head_values = piece_values[:, head * VALUE_WIDTH : (head + 1) * VALUE_WIDTH]
        scores = (
            jnp.einsum(
                "qd,kd->qk", plain_query[:, head], head_keys, preferred_element_type=jnp.float32
            )
            + jnp.einsum(
                "qd,kd->qk", query_rot[:, head], piece_rot, preferred_element_type=jnp.float32
            )
        ) * scale
        peak = jnp.max(scores, axis=1)
        factor = jnp.exp(most[head] - peak)
        weights = jnp.exp(scores - peak[:, None])
        new_total.append(total[head] * factor + jnp.sum(weights, axis=1))
        new_summed.append(
            summed[head] * factor[:, None]
            + jnp.dot(weights.astype(jnp.bfloat16), head_values, preferred_element_type=jnp.float32)
        )
        new_most.append(peak)
    total = jnp.stack(new_total)
    summed = jnp.stack(new_summed)
    attended = jnp.transpose((summed / total[..., None]).astype(jnp.bfloat16), (1, 0, 2)).reshape(
        tok_dev, heads_dev * VALUE_WIDTH
    )
    rows_dev = residual.shape[0]
    token_heads = lax.all_to_all(attended, "tp", split_axis=0, concat_axis=1, tiled=True)
    projected = jnp.dot(token_heads, out_weight, preferred_element_type=jnp.float32)
    hidden = (residual.astype(jnp.float32) + projected).astype(jnp.bfloat16)
    normed = norm_scale(hidden, ffn_gain).astype(jnp.bfloat16)
    top_count = routes.shape[1]
    experts_all = lax.axis_size(SP) * gate_weight.shape[0]
    capacity = min(rows_dev, max(2, rows_dev * top_count * 3 // (2 * experts_all)))
    flat_routes = routes.reshape(rows_dev * top_count)
    marks = (flat_routes[:, None] == jnp.arange(experts_all, dtype=jnp.int32)[None, :]).astype(
        jnp.int32
    )
    earlier = jnp.cumsum(marks, axis=0, dtype=jnp.int32) - marks
    slots = jnp.sum(earlier * marks, axis=1, dtype=jnp.int32)
    target = flat_routes * capacity + slots
    chosen = (
        target.reshape(rows_dev, top_count)[None, :, :]
        == jnp.arange(experts_all * capacity, dtype=jnp.int32)[:, None, None]
    )
    dispatch_table = jnp.sum(chosen.astype(jnp.bfloat16), axis=2)
    outgoing = jnp.dot(dispatch_table, normed, preferred_element_type=jnp.float32).astype(
        jnp.bfloat16
    )
    outgoing = outgoing.reshape(experts_all, capacity, model_width)
    gate_w = gate_weight[0]
    up_w = up_weight[0]
    down_w = down_weight[0]
    group = lax.axis_size("tp")
    gate_full, up_full, down_full = turned_gather((gate_w, up_w, down_w), "tp", (1, 1, 0))
    arrived = lax.all_to_all(outgoing, SP, split_axis=0, concat_axis=0, tiled=True)
    result_rows = expert_whole(
        arrived.reshape(experts_all * capacity, model_width), gate_full, up_full, down_full, group
    )
    returned = exchange_by_chip(
        result_rows.reshape(experts_all, capacity, model_width), ("sp_0", "sp_1"), (1, 0), 0, 0
    )
    picked = returned.reshape(experts_all * capacity, model_width)[target]
    picked = picked.reshape(rows_dev, top_count, model_width).astype(jnp.float32)
    return (hidden.astype(jnp.float32) + jnp.sum(route_weights[..., None] * picked, axis=1)).astype(
        jnp.bfloat16
    )


def solution(mesh):
    torus = Mesh(
        mesh.devices.reshape(mesh.shape["grp"], 16, 2, mesh.shape["tp"]),
        ("grp", "sp_0", "sp_1", "tp"),
    )
    placed = (
        P(GRP_SP, "tp"),
        P(GRP_SP, "tp"),
        P(GRP_SP, None),
        P(GRP_SP, None),
        P(),
        P(None, "tp"),
        P(None, "tp"),
        P(GRP_SP_TP, None),
        P(),
        P(),
        P(SP, None, "tp"),
        P(SP, None, "tp"),
        P(SP, "tp", None),
        P(GRP_SP_TP, None),
        P(GRP_SP_TP, None),
    )
    return jax.shard_map(
        on_device, mesh=torus, in_specs=placed, out_specs=P(GRP_SP_TP, None), check_vma=False
    )
```

profile of v0, /device:TPU:40, one launch (start us, length us, event | category | flops | bytes accessed | tf_op | source)
XLA Modules:
  0.0 310.2 jit_solution(7776849853484320127)
XLA Ops:
  6.6 0.8 convert_element_type.119
  7.3 1.0 fusion.74
  8.4 1.2 convolution_convert_fusion.5
  9.6 1.3 convolution_convert_fusion.6
  10.8 0.7 pad_maximum_fusion.1
  11.7 1.5 copy.71
  13.2 0.6 copy.70
  13.8 2.8 pad_maximum_fusion
  16.8 0.2 multiply_cosine_fusion.1
  17.0 0.1 copy.61
  17.2 0.1 convert_element_type.126
  17.3 52.1 %all_gather.10 = bf16[2560,128]{1,0:T(8,128)(2,1)S(1)} all-gather(bf16[80,128]{1,0:T(8,128)(2,1)S(1)} %convert_element_type.126), channel_id=1, replica_groups=mesh['grp'=2,'sp_0'=16,'sp_1'=2,'tp'=4] {'sp_0','sp_1'}, dimensions={0}, use_global_device_ids=true | all-gather | bytes 675840 | tf_op jit(solution)/shard_map/all_gather | solution.py:164
  69.4 0.5 reshape.301
  69.9 0.1 copy.60
  70.1 0.1 copy.65
  70.2 0.1 eq.37
  70.3 0.6 reduce-window.6
  70.9 0.2 slice_reduce_fusion
  71.1 0.1 bitcast_bitcast_fusion
  71.2 0.1 reduce_sum.74
  71.3 0.6 broadcast_multiply_fusion
  72.0 0.1 copy.69
  72.1 0.7 fusion.103
  72.8 2.3 fusion.95
  75.1 2.0 fusion.96
  77.1 21.7 %all-gather.3.cloned.1.call-done = bf16[5120,512]{1,0:T(8,128)(2,1)} async-done(((bf16[160,512]{1,0:T(8,128)(2,1)}), bf16[5120,512]{1,0:T(8,128)(2,1)}) %all-gather.3.cloned.1.call-update) | async-done | bytes 5242896 | tf_op jit(solution)/shard_map/all_gather | solution.py:24
  98.8 3.2 %fusion.104 = (f32[160]{0:T(256)S(1)}, f32[160,5120]{1,0:T(8,128)S(1)}) fusion(f32[160,5120]{1,0:T(8,128)} %fusion.95, bf16[160,1,128]{2,1,0:T(2,128)(2,1)S(1)} %copy-done.4, bf16[5120,512]{1,0:T(8,128)(2,1)} %all-gather.3.cloned.1.call-done), kind=kOutput, calls=%fused_computation.135 | convolution fusion | flops 212172640 | bytes 7905920 | tf_op jit(solution)/shard_map/qd,kd->qk/dot_general | solution.py:175
  102.0 0.6 fusion.10
  102.6 0.1 slice-done.1
  102.7 0.7 fusion.105
  103.4 0.6 fusion.8
  104.0 0.7 fusion.65
  104.8 0.7 fusion.55
  105.5 0.1 fusion.86
  105.7 0.7 all_to_all.23
  106.4 4.5 %all-to-all-start = ((bf16[4,40,256]{2,1,0:T(8,128)(2,1)}), bf16[4,40,256]{2,1,0:T(8,128)(2,1)S(1)}, u32[]{:S(2)}, u32[]{:S(2)}) async-start(bf16[4,40,256]{2,1,0:T(8,128)(2,1)} %all_to_all.23), calls=%async_computation | async-start | bytes 163840 | tf_op jit(solution)/shard_map/all_to_all | solution.py:197
  111.0 0.1 fusion.85
  111.0 5.6 %all-to-all-done = bf16[4,40,256]{2,1,0:T(8,128)(2,1)S(1)} async-done(((bf16[4,40,256]{2,1,0:T(8,128)(2,1)}), bf16[4,40,256]{2,1,0:T(8,128)(2,1)S(1)}, u32[]{:S(2)}, u32[]{:S(2)}) %all-to-all-start) | async-done | bytes 81952 | tf_op jit(solution)/shard_map/all_to_all | solution.py:197
  116.7 3.5 %multiply_reduce_fusion.1 = (f32[40]{0:T(128)S(1)}, f32[40,2048]{1,0:T(8,128)S(1)}) fusion(bf16[40,1024]{1,0:T(8,128)(2,1)S(1)} %bitcast.79, bf16[1024,2048]{1,0:T(8,128)(2,1)} %param.23, bf16[40,2048]{1,0:T(8,128)(2,1)S(1)} %copy-done.5), kind=kOutput, calls=%fused_computation.66 | convolution fusion | flops 168263648 | bytes 4767904 | tf_op jit(solution)/shard_map/dot_general | solution.py:198
  120.2 0.5 convolution_convert_fusion.4
  120.6 0.3 reshape.304
  120.9 63.1 %all_to_all.34 = bf16[32,7,2048]{2,1,0:T(8,128)(2,1)S(1)} all-to-all(bf16[32,7,2048]{2,1,0:T(8,128)(2,1)S(1)} %reshape.304), channel_id=1, replica_groups=mesh['grp'=2,'sp_0'=16,'sp_1'=2,'tp'=4] {'sp_0','sp_1'}, dimensions={0} | all-to-all | bytes 1835008 | tf_op jit(solution)/shard_map/all_to_all | solution.py:225
  184.0 0.3 reshape.305
  184.3 37.1 %all-gather.5.cloned.1.call-done = bf16[1024,6144]{1,0:T(8,128)(2,1)} async-done(((bf16[256,6144]{1,0:T(8,128)(2,1)}), bf16[1024,6144]{1,0:T(8,128)(2,1)}) %all-gather.5.cloned.1.call-update) | async-done | bytes 12582928 | tf_op jit(solution)/shard_map/all_gather | solution.py:34
  221.4 3.6 %fusion.44 = f32[224,1024]{1,0:T(8,128)S(1)} fusion(bf16[224,2048]{1,0:T(8,128)(2,1)S(1)} %reshape.305, bf16[1024,6144]{1,0:T(8,128)(2,1)} %all-gather.5.cloned.1.call-done), kind=kOutput, calls=%fused_computation.47 | convolution fusion | flops 939753472 | bytes 6029312 | tf_op jit(solution)/shard_map/dot_general | solution.py:103
  225.0 3.7 %fusion.47 = bf16[224,1024]{1,0:T(8,128)(2,1)S(1)} fusion(f32[224,1024]{1,0:T(8,128)S(1)} %fusion.44, bf16[224,2048]{1,0:T(8,128)(2,1)S(1)} %reshape.305, bf16[1024,6144]{1,0:T(8,128)(2,1)} %all-gather.5.cloned.1.call-done), kind=kOutput, calls=%fused_computation.48 | convolution fusion | flops 941588480 | bytes 6488064 | tf_op jit(solution)/shard_map/dot_general | solution.py:104
  228.8 1.6 fusion.19
  230.4 1.6 fusion.18
  232.0 1.6 fusion.16
  233.7 1.6 fusion.14
  235.3 0.3 reshape_reshape_reshape.6
  235.7 0.6 copy.72
  236.3 4.5 %all_to_all.35 = bf16[16,2,1,7,2048]{4,0,3,2,1:T(8,128)(2,1)S(1)} all-to-all(bf16[16,2,1,7,2048]{4,0,3,2,1:T(8,128)(2,1)S(1)} %copy.72), channel_id=1, replica_groups=mesh['grp'=2,'sp_0'=16,'sp_1'=2,'tp'=4] {'sp_1'}, dimensions={1} | all-to-all | bytes 1835008 | tf_op jit(solution)/shard_map/all_to_all | solution.py:58
  240.7 1.9 copy.73
  242.6 12.3 %all-to-all-start.3 = ((bf16[16,2,1,7,2048]{4,1,3,2,0:T(2,128)(2,1)}), bf16[16,2,1,7,2048]{4,1,3,2,0:T(2,128)(2,1)S(1)}, u32[]{:S(2)}, u32[]{:S(2)}) async-start(bf16[16,2,1,7,2048]{4,1,3,2,0:T(2,128)(2,1)} %copy.73), calls=%async_computation.3 | async-start | bytes 1835008 | tf_op jit(solution)/shard_map/all_to_all | solution.py:58
  255.0 0.1 mul.284
  255.1 0.1 copy.64
  255.2 44.4 %all-to-all-done.3 = bf16[16,2,1,7,2048]{4,1,3,2,0:T(2,128)(2,1)S(1)} async-done(((bf16[16,2,1,7,2048]{4,1,3,2,0:T(2,128)(2,1)}), bf16[16,2,1,7,2048]{4,1,3,2,0:T(2,128)(2,1)S(1)}, u32[]{:S(2)}, u32[]{:S(2)}) %all-to-all-start.3) | async-done | bytes 917536 | tf_op jit(solution)/shard_map/all_to_all | solution.py:58
  299.6 0.4 copy.74
  300.0 0.3 reshape_reshape_reshape.7
  300.3 1.0 gather_fusion
  301.3 0.4 reshape.309
  301.7 0.9 multiply_reduce_fusion
  302.7 0.7 add_convert_fusion
  (57 shorter events, 0.6 us)
Async XLA Ops:
  6.5 1.8 copy-start
  6.6 6.6 %copy-start.3 = (bf16[1,2048,256]{2,1,0:T(8,128)(2,1)S(1)}, bf16[1,2048,256]{2,1,0:T(8,128)(2,1)}, u32[]{:S(2)}) copy-start(bf16[1,2048,256]{2,1,0:T(8,128)(2,1)} %param.25) | copy-start | bytes 3145732
  6.6 92.2 %all-gather.3.cloned.1.call-start = ((), (), s32[]{:S(2)}) async-start(), calls=%async_computation.4 | async-start | bytes 5406720 | tf_op jit(solution)/shard_map/all_gather | solution.py:24
  11.6 209.8 %all-gather.5.cloned.1.call-start = ((), (), s32[]{:S(2)}) async-start(), calls=%async_computation.5 | async-start | bytes 15728640 | tf_op jit(solution)/shard_map/all_gather | solution.py:34
  13.8 2.9 copy-start.9
  16.7 53.2 %copy-start.8 = (bf16[160,128]{1,0:T(8,128)(2,1)S(1)}, bf16[160,128]{1,0:T(8,128)(2,1)}, u32[]{:S(2)}) copy-start(bf16[160,128]{1,0:T(8,128)(2,1)} %param.16) | copy-start | bytes 122884
  16.7 53.4 %copy-start.7 = (bf16[160,256]{1,0:T(8,128)(2,1)S(1)}, bf16[160,256]{1,0:T(8,128)(2,1)}, u32[]{:S(2)}) copy-start(bf16[160,256]{1,0:T(8,128)(2,1)} %param.15) | copy-start | bytes 245764
  16.7 53.4 %copy-start.11 = (s32[40,4]{0,1:T(4,128)S(1)}, s32[40,4]{0,1:T(4,128)}, u32[]{:S(2)}) copy-start(s32[40,4]{0,1:T(4,128)} %param.28) | copy-start | bytes 1924
  16.7 55.4 %copy-start.10 = (bf16[2048]{0:T(1024)(128)(2,1)S(1)}, bf16[2048]{0:T(1024)(128)(2,1)}, u32[]{:S(2)}) copy-start(bf16[2048]{0:T(1024)(128)(2,1)} %param.24) | copy-start | bytes 12292
  69.9 3.0 copy-start.2
  75.1 23.7 %copy-start.4 = (bf16[160,1,128]{2,1,0:T(2,128)(2,1)S(1)}, bf16[160,1,128]{2,1,0:T(2,128)(2,1)}, u32[]{:S(2)}) copy-start(bf16[160,1,128]{2,1,0:T(2,128)(2,1)} %get-tuple-element.12) | copy-start | bytes 122884
  98.8 3.8 %slice-start = ((s8[5242880]{0:T(1024)(128)(4,1)}), s8[4194304]{0:T(1024)(128)(4,1)S(1)}, s32[]{:S(2)}) async-start(s8[5242880]{0:T(1024)(128)(4,1)} %bitcast.73), calls=%async_computation.6 | async-start | bytes 8388608
  98.8 3.9 %slice-start.1 = ((s8[5242880]{0:T(1024)(128)(4,1)}), s8[1048576]{0:T(1024)(128)(4,1)S(1)}, s32[]{:S(2)}) async-start(s8[5242880]{0:T(1024)(128)(4,1)} %bitcast.73), calls=%async_computation.7 | async-start | bytes 2097152
  104.8 11.9 %copy-start.5 = (bf16[40,2048]{1,0:T(8,128)(2,1)S(1)}, bf16[40,2048]{1,0:T(8,128)(2,1)}, u32[]{:S(2)}) copy-start(bf16[40,2048]{1,0:T(8,128)(2,1)} %param.22) | copy-start | bytes 491524
  106.4 10.3 %all-to-all-start = ((bf16[4,40,256]{2,1,0:T(8,128)(2,1)}), bf16[4,40,256]{2,1,0:T(8,128)(2,1)S(1)}, u32[]{:S(2)}, u32[]{:S(2)}) async-start(bf16[4,40,256]{2,1,0:T(8,128)(2,1)} %all_to_all.23), calls=%async_computation | async-start | bytes 163840 | tf_op jit(solution)/shard_map/all_to_all | solution.py:197
  235.6 19.3 %copy-start.6 = (s32[40,4]{1,0:T(8,128)S(1)}, s32[40,4]{1,0:T(8,128)}, u32[]{:S(2)}) copy-start(s32[40,4]{1,0:T(8,128)} %get-tuple-element.19) | copy-start | bytes 1924
  235.7 19.4 %copy-start.12 = (f32[40,4]{0,1:T(4,128)S(1)}, f32[40,4]{0,1:T(4,128)}, u32[]{:S(2)}) copy-start(f32[40,4]{0,1:T(4,128)} %param.29) | copy-start | bytes 1924
  242.6 57.0 %all-to-all-start.3 = ((bf16[16,2,1,7,2048]{4,1,3,2,0:T(2,128)(2,1)}), bf16[16,2,1,7,2048]{4,1,3,2,0:T(2,128)(2,1)S(1)}, u32[]{:S(2)}, u32[]{:S(2)}) async-start(bf16[16,2,1,7,2048]{4,1,3,2,0:T(2,128)(2,1)} %copy.73), calls=%async_computation.3 | async-start | bytes 1835008 | tf_op jit(solution)/shard_map/all_to_all | solution.py:58
  300.3 3.1 %copy-start.1 = (bf16[512,256]{1,0:T(8,128)(2,1)S(1)}, bf16[512,256]{1,0:T(8,128)(2,1)}, u32[]{:S(2)}) copy-start(bf16[512,256]{1,0:T(8,128)(2,1)} %param.21) | copy-start | bytes 786436
Sparse Core Ops, SparseCore 0:
  11.7 87.0 all-gather.2
  100.6 120.7 all-gather.4
where the time goes:
time: 312 us; the launch traced here: 310 us
  blocking collectives  120 us (38%)
  waiting for transfers between devices  109 us (35%)
  matrix products  29.9 us (10%)
  starting transfers between devices  17 us (5%)
  between operations  13.9 us (4%)
  local copies, waits for them, and re-layouts  10.8 us (3%)
  other arithmetic  10.1 us (3%)
    all_to_all x1, blocking collectives, on_device(): lax.all_to_all(outgoing, SP, split_axis=0, concat_axis=0, tiled=True)  63.1 us
    all_gather x1, blocking collectives, on_device(): lax.all_gather(key_pairs, SP, axis=0, tiled=True)  52.1 us
    all_to_all x1, waiting for transfers between devices, moved_by_axis(): result = lax.all_to_all(result, axes[k], k, k, tiled=True)  44.4 us
    all_gather x1, waiting for transfers between devices, turned_gather(): lax.all_gather(both, axis, axis=0, tiled=True)  37.1 us
    all_gather x1, waiting for transfers between devices, sent_together(): lax.all_gather(both, axis, axis=dim, tiled=True)  21.7 us
    all_to_all x1, starting transfers between devices, moved_by_axis(): result = lax.all_to_all(result, axes[k], k, k, tiled=True)  12.3 us
    dot_general x4, matrix products, expert_whole(): jnp.dot(active[:, index * piece:(index + 1) * piece], down_w[index * piec...  6.55 us
  transfers between devices with their start and end apart: 4, of which 4 were waited for; matrix products, arithmetic and copies ran while one was open for 8% of the time, Pallas kernels for 0%

commit v1 on v0

v1 whole, which is shorter than its diff:
```python
import functools

import jax
import jax.numpy as jnp
from jax import lax
from jax.experimental import pallas as pl
from jax.experimental.pallas import tpu as pltpu
from jax.sharding import Mesh
from jax.sharding import PartitionSpec as P

PLAIN_HEAD_WIDTH = 128
QK_ROPE = 64
VALUE_WIDTH = 128
GRID_W = 64
SP = ("sp_0", "sp_1")
GRP_SP = ("grp", "sp_0", "sp_1")
GRP_SP_TP = ("grp", "sp_0", "sp_1", "tp")
MESH = pl.DeviceIdType.MESH

theta = 10000.0
eps = 1e-06
limit = 7.0
slope = 1.702

SLOTS = 8
HALF = 64
SPLIT = 2


def sent_together(arrays, axis, dim, along):
    both = jnp.concatenate(arrays, axis=along)
    result, at, finished = (lax.all_gather(both, axis, axis=dim, tiled=True), 0, [])
    for a in arrays:
        finished.append(lax.slice_in_dim(result, at, at + a.shape[along], axis=along))
        at += a.shape[along]
    return tuple(finished)


def turn(vector, row_shift, col_shift):
    width = vector.shape[-1]
    count = width // 4
    half = width // 2
    freqs = theta ** (-jnp.arange(count, dtype=jnp.float32) / count)
    extra = (1,) * (vector.ndim - 2)
    pieces = []
    for portion, shift in ((vector[..., :half], row_shift), (vector[..., half:], col_shift)):
        angle = (shift.astype(jnp.float32)[:, None] * freqs[None, :]).reshape(
            (shift.shape[0],) + extra + (count,)
        )
        lower = portion[..., :count]
        upper = portion[..., count:]
        pieces.append(
            jnp.concatenate(
                [
                    lower * jnp.cos(angle) - upper * jnp.sin(angle),
                    lower * jnp.sin(angle) + upper * jnp.cos(angle),
                ],
                axis=-1,
            )
        )
    return jnp.concatenate(pieces, axis=-1)


def norm_scale(values, gain):
    wide = values.astype(jnp.float32)
    return (
        wide
        * lax.rsqrt(jnp.mean(wide * wide, axis=-1, keepdims=True) + eps)
        * gain.astype(jnp.float32)
    )


def greet(peers):
    barrier = pltpu.get_barrier_semaphore()
    for peer in peers:
        pl.semaphore_signal(barrier, inc=1, device_id=peer, device_id_type=MESH)
    pl.semaphore_wait(barrier, len(peers))


def places():
    z = lax.axis_index("sp_0")
    c = lax.axis_index("sp_1")
    x = lax.axis_index("tp")
    count = lax.axis_size("sp_0")
    after = lax.rem(z + 1, count)
    before = lax.rem(z + count - 1, count)
    mirror = lax.axis_size("tp") - 1 - x
    ring = ({"sp_0": after}, {"sp_0": before})
    near = ({"sp_1": 1 - c}, {"tp": mirror}, {"sp_1": 1 - c, "tp": mirror})
    return z, c, ring, near


def matches(z, c, merged):
    row = lax.broadcasted_iota(jnp.int32, (4 * SLOTS, 2 * HALF), 0)
    lane = lax.broadcasted_iota(jnp.int32, (4 * SLOTS, 2 * HALF), 1)
    core = jnp.where(row < 2 * SLOTS, c, 1 - c)
    wanted = ((2 * z + core) * SLOTS + row % SLOTS).astype(jnp.float32)
    same = (row // SLOTS) % 2 == lane // HALF
    return [
        jnp.logical_and(same, jnp.broadcast_to(merged[k : k + 1], wanted.shape) == wanted)
        for k in range(4)
    ]


def merged_notes(first, second):
    return jnp.concatenate(
        [first[...].astype(jnp.float32)[:, :HALF], second[...].astype(jnp.float32)[:, :HALF]],
        axis=1,
    )


def dispatch_kernel(
    norm_ref,
    note_ref,
    sent_ref,
    notes_ref,
    blocks,
    notes,
    chosen,
    ring_send,
    ring_recv,
    note_send,
    note_recv,
    near_send,
    near_recv,
    own_sem,
):
    z, c, ring, near = places()
    steps, _, width = blocks.shape
    rows = norm_ref.shape[0]
    part = width // SPLIT
    last = (steps - 1, steps - 2)
    for j in range(steps):
        for d in range(2):
            blocks[j, d * HALF + rows : (d + 1) * HALF] = jnp.zeros(
                (HALF - rows, width), blocks.dtype
            )
    greet((*ring, *near))

    def ring_copy(d, j, h):
        columns = pl.ds(h * part, part)
        span = pl.ds(d * HALF, rows)
        source = norm_ref.at[:, columns] if j == 0 else blocks.at[j - 1, span, columns]
        return pltpu.make_async_remote_copy(
            src_ref=source,
            dst_ref=blocks.at[j, span, columns],
            send_sem=ring_send.at[d, j, h],
            recv_sem=ring_recv.at[d, j, h],
            device_id=ring[d],
            device_id_type=MESH,
        )

    def note_copy(d, j):
        return pltpu.make_async_remote_copy(
            src_ref=note_ref if j == 0 else notes.at[d, j - 1],
            dst_ref=notes.at[d, j],
            send_sem=note_send.at[d, j],
            recv_sem=note_recv.at[d, j],
            device_id=ring[d],
            device_id_type=MESH,
        )

    def near_copy(j, q):
        return pltpu.make_async_remote_copy(
            src_ref=chosen.at[j, pl.ds((q % 2) * 2 * SLOTS, 2 * SLOTS)],
            dst_ref=sent_ref.at[j, pl.ds(q * 2 * SLOTS, 2 * SLOTS)],
            send_sem=near_send.at[j, q - 1],
            recv_sem=near_recv.at[j, q - 1],
            device_id=near[q - 1],
            device_id_type=MESH,
        )

    def own_copy(j):
        return pltpu.make_async_copy(
            chosen.at[j, pl.ds(0, 2 * SLOTS)], sent_ref.at[j, pl.ds(0, 2 * SLOTS)], own_sem.at[j]
        )

    for d in range(2):
        note_copy(d, 0).start()
    for h in range(SPLIT):
        for d in range(2):
            ring_copy(d, 0, h).start()
    blocks[steps - 1, HALF : HALF + rows] = norm_ref[...]
    notes[1, steps - 1] = note_ref[...]
    for j in range(steps):
        for d in range(2):
            if j <= last[d]:
                note_copy(d, j).wait_recv()
                if j < last[d]:
                    note_copy(d, j + 1).start()
        for h in range(SPLIT):
            for d in range(2):
                if j <= last[d]:
                    ring_copy(d, j, h).wait_recv()
                    if j < last[d]:
                        ring_copy(d, j + 1, h).start()
        merged = merged_notes(notes.at[0, j], notes.at[1, j])
        notes_ref[j] = merged
        found = matches(z, c, merged)
        picks = sum(m.astype(jnp.float32) for m in found).astype(jnp.bfloat16)
        chosen[j] = jnp.dot(picks, blocks[j], preferred_element_type=jnp.float32).astype(
            jnp.bfloat16
        )
        own_copy(j).start()
        for q in (2, 3, 1):
            near_copy(j, q).start()
    for j in range(steps):
        for d in range(2):
            if j <= last[d]:
                note_copy(d, j).wait_send()
                for h in range(SPLIT):
                    ring_copy(d, j, h).wait_send()
        own_copy(j).wait()
        for q in (1, 2, 3):
            near_copy(j, q).wait()


def dispatch(normed, note, steps):
    rows, width = normed.shape
    return pl.pallas_call(
        dispatch_kernel,
        name="dispatch",
        out_shape=(
            jax.ShapeDtypeStruct((steps, 8 * SLOTS, width), jnp.bfloat16),
            jax.ShapeDtypeStruct((steps, 16, 2 * HALF), jnp.float32),
        ),
        in_specs=[pl.BlockSpec(memory_space=pltpu.VMEM)] * 2,
        out_specs=(
            pl.BlockSpec(memory_space=pl.ANY),
            pl.BlockSpec(memory_space=pltpu.VMEM),
        ),
        scratch_shapes=[
            pltpu.VMEM((steps, 2 * HALF, width), jnp.bfloat16),
            pltpu.VMEM((2, steps, 16, 2 * HALF), jnp.bfloat16),
            pltpu.VMEM((steps, 4 * SLOTS, width), jnp.bfloat16),
            pltpu.SemaphoreType.DMA((2, steps, SPLIT)),
            pltpu.SemaphoreType.DMA((2, steps, SPLIT)),
            pltpu.SemaphoreType.DMA((2, steps)),
            pltpu.SemaphoreType.DMA((2, steps)),
            pltpu.SemaphoreType.DMA((steps, 3)),
            pltpu.SemaphoreType.DMA((steps, 3)),
            pltpu.SemaphoreType.DMA((steps,)),
        ],
        compiler_params=pltpu.CompilerParams(
            collective_id=1, has_side_effects=True, vmem_limit_bytes=40 * 2**20
        ),
        cost_estimate=pl.CostEstimate(
            flops=30_000_000_000, bytes_accessed=8_000_000, transcendentals=0
        ),
    )(normed, note)


def combine_kernel(
    sent_ref,
    notes_ref,
    gate_ref,
    up_ref,
    down_ref,
    gate2_ref,
    up2_ref,
    down2_ref,
    out_ref,
    taken,
    gate_w,
    up_w,
    down_w,
    product,
    back,
    token,
    own,
    arrive,
    leave,
    load_sem,
    weight_sem,
    near_send,
    near_recv,
    ring_send,
    ring_recv,
):
    z, c, ring, near = places()
    steps, taken_rows, width = taken.shape
    rows = out_ref.shape[0]
    part = width // SPLIT
    span = 2 * SLOTS
    group = steps // 2
    halves = ((group, steps), (0, group))
    loads = [
        pltpu.make_async_copy(
            sent_ref.at[pl.ds(a, b - a)], taken.at[pl.ds(a, b - a)], load_sem.at[i]
        )
        for i, (a, b) in enumerate(halves)
    ]
    weights = [
        pltpu.make_async_copy(source, target.at[i // 3], weight_sem.at[i])
        for i, (source, target) in enumerate(
            (
                (gate_ref, gate_w),
                (up_ref, up_w),
                (down_ref, down_w),
                (gate2_ref, gate_w),
                (up2_ref, up_w),
                (down2_ref, down_w),
            )
        )
    ]
    loads[0].start()
    for w in weights[:2]:
        w.start()
    loads[1].start()
    for w in weights[2:]:
        w.start()
    greet((*ring, *near))

    def near_copy(j, q):
        return pltpu.make_async_remote_copy(
            src_ref=product.at[j, pl.ds(q * span, span)],
            dst_ref=back.at[j, pl.ds(q * span, span)],
            send_sem=near_send.at[j, q - 1],
            recv_sem=near_recv.at[j, q - 1],
            device_id=near[q - 1],
            device_id_type=MESH,
        )

    def ring_copy(d, j, h):
        columns = pl.ds(h * part, part)
        slot = j - 1 if j > 0 else steps - 1
        return pltpu.make_async_remote_copy(
            src_ref=leave.at[d, j, :, columns],
            dst_ref=arrive.at[d, slot, :, columns],
            send_sem=ring_send.at[d, j, h],
            recv_sem=ring_recv.at[d, j, h],
            device_id=ring[1 - d],
            device_id_type=MESH,
        )

    for i, (a, b) in enumerate(halves):
        loads[i].wait()
        x = taken[a:b].reshape((b - a) * taken_rows, width)
        result = None
        for half in range(2):
            if i == 0:
                weights[3 * half].wait()
            gate = jnp.minimum(
                jnp.dot(x, gate_w[half], preferred_element_type=jnp.float32), limit
            )
            if i == 0:
                weights[3 * half + 1].wait()
            up = jnp.clip(
                jnp.dot(x, up_w[half], preferred_element_type=jnp.float32), -limit, limit
            )
            active = ((up + 1.0) * gate * jax.nn.sigmoid(slope * gate)).astype(jnp.bfloat16)
            if i == 0:
                weights[3 * half + 2].wait()
            term = jnp.dot(active, down_w[half], preferred_element_type=jnp.float32)
            result = term if result is None else result + term
        product[a:b] = result.astype(jnp.bfloat16).reshape(b - a, taken_rows, width)
        for j in range(b - 1, a - 1, -1):
            for q in (2, 3, 1):
                near_copy(j, q).start()
            back[j, 0:span] = product[j, 0:span]

    first = (steps - 1, steps - 2)
    for j in range(steps - 1, -1, -1):
        merged = notes_ref[j]
        found = matches(z, c, merged)
        tables = []
        for base in (4, 8):
            table = sum(
                jnp.where(m, jnp.broadcast_to(merged[base + k : base + k + 1], m.shape), 0.0)
                for k, m in enumerate(found)
            )
            flat = jnp.transpose(table)
            tables.append(jnp.concatenate([flat, flat], axis=1).astype(jnp.bfloat16))
        for q in (1, 2, 3):
            near_copy(j, q).wait_recv()
        token[...] = jnp.dot(tables[0], back[j], preferred_element_type=jnp.float32) + jnp.dot(
            tables[1], back[j], preferred_element_type=jnp.float32
        )
        if j == steps - 1:
            own[...] = token[HALF : HALF + rows]
        for h in range(SPLIT):
            columns = slice(h * part, (h + 1) * part)
            for d in range(2):
                if j > first[d]:
                    continue
                total = token[d * HALF : d * HALF + rows, columns]
                if j < first[d]:
                    ring_copy(d, j + 1, h).wait_recv()
                    total = total + arrive[d, j, :, columns].astype(jnp.float32)
                leave[d, j, :, columns] = total.astype(jnp.bfloat16)
                ring_copy(d, j, h).start()
    for h in range(SPLIT):
        columns = slice(h * part, (h + 1) * part)
        for d in range(2):
            ring_copy(d, 0, h).wait_recv()
        out_ref[:, columns] = (
            own[:, columns]
            + arrive[0, steps - 1, :, columns].astype(jnp.float32)
            + arrive[1, steps - 1, :, columns].astype(jnp.float32)
        )
    for j in range(steps):
        for q in (1, 2, 3):
            near_copy(j, q).wait_send()
        for d in range(2):
            if j <= first[d]:
                for h in range(SPLIT):
                    ring_copy(d, j, h).wait_send()


def combine(sent, notes, weights, rows):
    steps, taken_rows, width = sent.shape
    hidden_units = weights[0].shape[1]
    any_space = pl.BlockSpec(memory_space=pl.ANY)
    vmem = pl.BlockSpec(memory_space=pltpu.VMEM)
    bf16 = jnp.bfloat16
    return pl.pallas_call(
        combine_kernel,
        name="combine",
        out_shape=jax.ShapeDtypeStruct((rows, width), jnp.float32),
        in_specs=[any_space, vmem] + [any_space] * 6,
        out_specs=vmem,
        scratch_shapes=[
            pltpu.VMEM((steps, taken_rows, width), bf16),
            pltpu.VMEM((2, width, hidden_units), bf16),
            pltpu.VMEM((2, width, hidden_units), bf16),
            pltpu.VMEM((2, hidden_units, width), bf16),
            pltpu.VMEM((steps, taken_rows, width), bf16),
            pltpu.VMEM((steps, taken_rows, width), bf16),
            pltpu.VMEM((2 * HALF, width), jnp.float32),
            pltpu.VMEM((rows, width), jnp.float32),
            pltpu.VMEM((2, steps, rows, width), bf16),
            pltpu.VMEM((2, steps, rows, width), bf16),
            pltpu.SemaphoreType.DMA((2,)),
            pltpu.SemaphoreType.DMA((6,)),
            pltpu.SemaphoreType.DMA((steps, 3)),
            pltpu.SemaphoreType.DMA((steps, 3)),
            pltpu.SemaphoreType.DMA((2, steps, SPLIT)),
            pltpu.SemaphoreType.DMA((2, steps, SPLIT)),
        ],
        compiler_params=pltpu.CompilerParams(
            collective_id=2, has_side_effects=True, vmem_limit_bytes=56 * 2**20
        ),
        cost_estimate=pl.CostEstimate(
            flops=30_000_000_000, bytes_accessed=8_000_000, transcendentals=0
        ),
    )(sent, notes, *weights)


def routing_note(routes, route_weights, experts):
    rows, top = routes.shape
    flat = routes.reshape(rows * top)
    marks = (flat[:, None] == jnp.arange(experts, dtype=jnp.int32)[None, :]).astype(jnp.int32)
    earlier = jnp.cumsum(marks, axis=0, dtype=jnp.int32) - marks
    slots = jnp.sum(earlier * marks, axis=1, dtype=jnp.int32)
    target = (flat * SLOTS + slots).reshape(rows, top)
    high = route_weights.astype(jnp.bfloat16)
    low = (route_weights - high.astype(jnp.float32)).astype(jnp.bfloat16)
    parts = jnp.concatenate([target.astype(jnp.bfloat16), high, low], axis=1).T
    return jnp.pad(
        parts, ((0, 16 - 3 * top), (0, 2 * HALF - rows)), constant_values=-1.0
    )


def on_device(
    query_plain,
    query_turn,
    latent,
    key_turn,
    latent_norm_scale,
    plain_key_matrix,
    value_matrix,
    residual,
    out_weight,
    ffn_gain,
    gate_weight,
    up_weight,
    down_weight,
    routes,
    route_weights,
):
    tok_dev = latent.shape[0]
    heads_dev = query_plain.shape[1] // PLAIN_HEAD_WIDTH
    tp = lax.axis_size("tp")
    swap = [(i, i ^ 1) for i in range(tp)]
    own_weights = (gate_weight[0], up_weight[0], down_weight[0])
    other_weights = tuple(lax.ppermute(w, "tp", swap) for w in own_weights)
    experts_all = lax.axis_size(SP) * gate_weight.shape[0]
    note = routing_note(routes, route_weights, experts_all)
    place = lax.axis_index(SP) * tok_dev + jnp.arange(tok_dev, dtype=jnp.int32)
    grid_row = place // GRID_W
    grid_col = place % GRID_W
    normed_latent = norm_scale(latent, latent_norm_scale).astype(jnp.bfloat16)
    key_plain = jnp.dot(normed_latent, plain_key_matrix, preferred_element_type=jnp.float32).astype(
        jnp.bfloat16
    )
    values = jnp.dot(normed_latent, value_matrix, preferred_element_type=jnp.float32).astype(
        jnp.bfloat16
    )
    key_rot = turn(key_turn.astype(jnp.float32), grid_row, grid_col).astype(jnp.bfloat16)
    key_pairs = key_rot.reshape(tok_dev // 2, 2 * QK_ROPE)
    query_rot = turn(
        query_turn.astype(jnp.float32).reshape(tok_dev, heads_dev, QK_ROPE), grid_row, grid_col
    ).astype(jnp.bfloat16)
    plain_query = query_plain.reshape(tok_dev, heads_dev, PLAIN_HEAD_WIDTH)
    scale = (PLAIN_HEAD_WIDTH + QK_ROPE) ** (-0.5)
    piece_keys, piece_values, piece_pairs = (
        *sent_together((key_plain, values), SP, 0, 1),
        lax.all_gather(key_pairs, SP, axis=0, tiled=True),
    )
    count = piece_keys.shape[0]
    piece_rot = piece_pairs.reshape(count, QK_ROPE)
    new_total = []
    new_summed = []
    for head in range(heads_dev):
        head_keys = piece_keys[:, head * PLAIN_HEAD_WIDTH : (head + 1) * PLAIN_HEAD_WIDTH]
        head_values = piece_values[:, head * VALUE_WIDTH : (head + 1) * VALUE_WIDTH]
        scores = (
            jnp.einsum(
                "qd,kd->qk", plain_query[:, head], head_keys, preferred_element_type=jnp.float32
            )
            + jnp.einsum(
                "qd,kd->qk", query_rot[:, head], piece_rot, preferred_element_type=jnp.float32
            )
        ) * scale
        peak = jnp.max(scores, axis=1)
        weights = jnp.exp(scores - peak[:, None])
        new_total.append(jnp.sum(weights, axis=1))
        new_summed.append(
            jnp.dot(weights.astype(jnp.bfloat16), head_values, preferred_element_type=jnp.float32)
        )
    total = jnp.stack(new_total)
    summed = jnp.stack(new_summed)
    attended = jnp.transpose((summed / total[..., None]).astype(jnp.bfloat16), (1, 0, 2)).reshape(
        tok_dev, heads_dev * VALUE_WIDTH
    )
    rows_dev = residual.shape[0]
    token_heads = lax.all_to_all(attended, "tp", split_axis=0, concat_axis=1, tiled=True)
    projected = jnp.dot(token_heads, out_weight, preferred_element_type=jnp.float32)
    hidden = (residual.astype(jnp.float32) + projected).astype(jnp.bfloat16)
    normed = norm_scale(hidden, ffn_gain).astype(jnp.bfloat16)
    sent, notes = dispatch(normed, note, lax.axis_size("sp_0") // 2)
    mixed = combine(sent, notes, (*own_weights, *other_weights), rows_dev)
    return (hidden.astype(jnp.float32) + mixed).astype(jnp.bfloat16)


def solution(mesh):
    torus = Mesh(
        mesh.devices.reshape(mesh.shape["grp"], mesh.shape["sp"] // 2, 2, mesh.shape["tp"]),
        ("grp", "sp_0", "sp_1", "tp"),
    )
    placed = (
        P(GRP_SP, "tp"),
        P(GRP_SP, "tp"),
        P(GRP_SP, None),
        P(GRP_SP, None),
        P(),
        P(None, "tp"),
        P(None, "tp"),
        P(GRP_SP_TP, None),
        P(),
        P(),
        P(SP, None, "tp"),
        P(SP, None, "tp"),
        P(SP, "tp", None),
        P(GRP_SP_TP, None),
        P(GRP_SP_TP, None),
    )
    return jax.shard_map(
        on_device, mesh=torus, in_specs=placed, out_specs=P(GRP_SP_TP, None), check_vma=False
    )
```

time: 312 us -> 224 us (0.72)
  Pallas kernels: 0 us -> 92.4 us
  waiting for transfers between devices: 109 us -> 25 us
  blocking collectives: 120 us -> 52 us
  matrix products: 29.9 us -> 15.2 us
  starting transfers between devices: 17 us -> 8.17 us
    pallas_call x0 -> x2, Pallas kernels: none -> 92.4 us  [the longest x1 49.9 us: combine(): pl.pallas_call(combine_kernel, name='combine', out_shape=jax.ShapeDtypeSt...]
    all_to_all x2 -> x0, blocking collectives: 67.6 us -> none  [the longest x1 63.1 us: on_device(): lax.all_to_all(outgoing, SP, split_axis=0, concat_axis=0, tiled=True)]
    all_to_all x1 -> x0, waiting for transfers between devices: 44.4 us -> none  [moved_by_axis(): result = lax.all_to_all(result, axes[k], k, k, tiled=True)]
    all_gather x1 -> x0, waiting for transfers between devices: 37.1 us -> none  [turned_gather(): lax.all_gather(both, axis, axis=0, tiled=True)]
    dot_general x7 -> x0, matrix products: 14.3 us -> none  [the longest x4 6.55 us: expert_whole(): jnp.dot(active[:, index * piece:(index + 1) * piece], down_w[index * piec...]
    all_to_all x1 -> x0, starting transfers between devices: 12.3 us -> none  [moved_by_axis(): result = lax.all_to_all(result, axes[k], k, k, tiled=True)]
    ppermute x0 -> x3, starting transfers between devices: none -> 3.78 us  [on_device(): other_weights = tuple((lax.ppermute(w, 'tp', swap) for w in own_weights))]
  transfers between devices with their start and end apart: 4 -> 5, of which waited for: 4 -> 2; matrix products, arithmetic and copies ran while one was open for 8% -> 10% of each run, Pallas kernels for 0% -> 19%
where the time goes in v1:
time: 224 us; the launch traced here: 223 us
  Pallas kernels  92.4 us (41%)
  blocking collectives  52 us (23%)
  waiting for transfers between devices  25 us (11%)
  matrix products  15.2 us (7%)
  between operations  13.7 us (6%)
  other arithmetic  8.8 us (4%)
  starting transfers between devices  8.17 us (4%)
  local copies, waits for them, and re-layouts  7.75 us (3%)
    all_gather x1, blocking collectives, on_device(): lax.all_gather(key_pairs, SP, axis=0, tiled=True)  52 us
    pallas_call x1, Pallas kernels, combine(): pl.pallas_call(combine_kernel, name='combine', out_shape=jax.ShapeDtypeSt...  49.9 us
    pallas_call x1, Pallas kernels, dispatch(): pl.pallas_call(dispatch_kernel, name='dispatch', out_shape=(jax.ShapeDtyp...  42.6 us
    all_gather x1, waiting for transfers between devices, sent_together(): lax.all_gather(both, axis, axis=dim, tiled=True)  19.3 us
    all_to_all x1, waiting for transfers between devices, on_device(): lax.all_to_all(attended, 'tp', split_axis=0, concat_axis=1, tiled=True)  5.68 us
  transfers between devices with their start and end apart: 5, of which 2 were waited for; matrix products, arithmetic and copies ran while one was open for 10% of the time, Pallas kernels for 19%

profile of v1, /device:TPU:40, one launch (start us, length us, event | category | flops | bytes accessed | tf_op | source)
XLA Modules:
  0.0 223.1 jit_solution(6769887890734388776)
XLA Ops:
  6.5 0.0 copy-start
  6.6 0.0 all-gather.2.cloned.1.call-start
  6.6 1.1 fusion.30
  7.7 0.7 convert_element_type.89
  8.3 0.0 copy-done
  8.3 1.2 convolution_convert_fusion
  9.5 1.3 convolution_convert_fusion.1
  10.8 0.7 pad_maximum_fusion
  11.5 0.1 all-gather.2.cloned.1.call-update
  11.5 1.8 collective-permute-start
  13.3 0.4 collective-permute-start.1
  13.7 1.6 collective-permute-start.2
  15.3 0.7 convert_element_type.102
  16.0 0.8 copy.32
  16.8 0.1 eq.24
  16.9 0.6 reduce-window.6
  17.5 0.2 slice_reduce_fusion
  17.7 0.1 bitcast_bitcast_fusion
  17.8 0.1 reduce_sum.52
  17.9 0.1 copy.35
  18.0 0.9 copy.28
  18.9 0.8 convert_element_type.95
  19.7 0.2 multiply_cosine_fusion.1
  20.0 0.1 copy.29
  20.1 0.1 convert_element_type.96
  20.2 0.9 reshape.196
  21.1 52.0 %all_gather.7 = bf16[2560,128]{1,0:T(8,128)(2,1)S(1)} all-gather(bf16[80,128]{1,0:T(8,128)(2,1)S(1)} %convert_element_type.96), channel_id=1, replica_groups=mesh['grp'=2,'sp_0'=16,'sp_1'=2,'tp'=4] {'sp_0','sp_1'}, dimensions={0}, use_global_device_ids=true | all-gather | bytes 675840 | tf_op jit(solution)/shard_map/all_gather | solution.py:508
  73.1 0.5 reshape.199
  73.6 0.0 copy-start.3
  73.6 0.0 copy-done.8
  73.6 0.7 subtract_convert_fusion.4
  74.4 0.0 copy-done.6
  74.4 0.8 fusion.48
  75.2 0.0 copy-done.3
  75.2 2.3 %fusion.43 = f32[160,5120]{1,0:T(8,128)} fusion(bf16[5120,64]{1,0:T(8,128)(2,1)S(1)} %reshape.199, bf16[160,2,64]{0,2,1:T(8,128)(2,1)S(1)} %pad_maximum_fusion.1), kind=kOutput, calls=%fused_computation.51 | convolution fusion | flops 104857600 | bytes 4620288 | tf_op jit(solution)/shard_map/qd,kd->qk/dot_general | solution.py:521
  77.5 1.9 fusion.44
  79.4 19.3 %all-gather.2.cloned.1.call-done = bf16[5120,512]{1,0:T(8,128)(2,1)} async-done(((bf16[160,512]{1,0:T(8,128)(2,1)}), bf16[5120,512]{1,0:T(8,128)(2,1)}) %all-gather.2.cloned.1.call-update) | async-done | bytes 5242896 | tf_op jit(solution)/shard_map/all_gather | solution.py:32
  98.7 3.2 %fusion.49 = (f32[160]{0:T(256)S(1)}, f32[160,5120]{1,0:T(8,128)S(1)}) fusion(f32[160,5120]{1,0:T(8,128)} %fusion.43, bf16[160,1,128]{2,1,0:T(2,128)(2,1)} %get-tuple-element.18, bf16[5120,512]{1,0:T(8,128)(2,1)} %all-gather.2.cloned.1.call-done), kind=kOutput, calls=%fused_computation.89 | convolution fusion | flops 212172640 | bytes 7946880 | tf_op jit(solution)/shard_map/qd,kd->qk/dot_general | solution.py:518
  102.0 0.0 copy-start.4
  102.0 0.6 fusion.6
  102.6 0.0 slice-done
  102.6 0.1 slice-done.1
  102.7 0.4 copy-done.4
  103.0 0.7 fusion.50
  103.7 0.6 fusion.4
  104.3 0.7 fusion.25
  105.1 0.0 copy-start.5
  105.1 0.7 fusion.20
  105.9 0.1 fusion.34
  106.0 0.1 copy.30
  106.1 0.7 all_to_all.14
  106.7 4.4 %all-to-all-start = ((bf16[4,40,256]{2,1,0:T(8,128)(2,1)}), bf16[4,40,256]{2,1,0:T(8,128)(2,1)S(1)}, u32[]{:S(2)}, u32[]{:S(2)}) async-start(bf16[4,40,256]{2,1,0:T(8,128)(2,1)} %all_to_all.14), calls=%async_computation | async-start | bytes 163840 | tf_op jit(solution)/shard_map/all_to_all | solution.py:537
  111.1 0.0 copy-done.7
  111.2 5.7 %all-to-all-done = bf16[4,40,256]{2,1,0:T(8,128)(2,1)S(1)} async-done(((bf16[4,40,256]{2,1,0:T(8,128)(2,1)}), bf16[4,40,256]{2,1,0:T(8,128)(2,1)S(1)}, u32[]{:S(2)}, u32[]{:S(2)}) %all-to-all-start) | async-done | bytes 81952 | tf_op jit(solution)/shard_map/all_to_all | solution.py:537
  116.9 3.1 %multiply_reduce_fusion = (f32[40]{0:T(128)S(1)}, f32[40,2048]{1,0:T(8,128)S(1)}) fusion(bf16[40,1024]{1,0:T(8,128)(2,1)S(1)} %bitcast.67, bf16[1024,2048]{1,0:T(8,128)(2,1)} %param.23, bf16[40,2048]{1,0:T(8,128)(2,1)S(1)} %copy-done.5), kind=kOutput, calls=%fused_computation.34 | convolution fusion | flops 168263648 | bytes 4767904 | tf_op jit(solution)/shard_map/dot_general | solution.py:538
  120.0 0.1 multiply_convert_fusion.norm_ref
  120.1 42.6 %dispatch.1 = (bf16[8,64,2048]{2,1,0:T(8,128)(2,1)S(1)}, f32[8,16,128]{2,1,0:T(8,128)S(1)}) custom-call(bf16[40,2048]{1,0:T(8,128)(2,1)S(1)} %multiply_convert_fusion.norm_ref, bf16[16,128]{1,0:T(8,128)(2,1)S(1)} %pad.9.note_ref), custom_call_target="tpu_custom_call" | custom-call | flops 30000001024 | bytes 8000000 | tf_op jit(solution)/shard_map/dispatch/pallas_call | solution.py:220
  162.7 1.3 copy-done.1
  164.0 0.6 copy-done.2
  164.7 0.0 collective-permute-done.gate2_ref
  164.7 0.0 collective-permute-done.1.up2_ref
  164.7 0.0 collective-permute-done.2.down2_ref
  164.7 49.9 %combine.1 = f32[40,2048]{1,0:T(8,128)} custom-call(bf16[8,64,2048]{2,1,0:T(8,128)(2,1)} %copy-done.1, f32[8,16,128]{2,1,0:T(8,128)} %copy-done.2, bf16[2048,256]{1,0:T(8,128)(2,1)} %bitcast.72, bf16[2048,256]{1,0:T(8,128)(2,1)} %bitcast.74, bf16[256,2048]{1,0:T(8,128)(2,1)} %bitcast.76, bf16[2048,256]{1,0:T(8,128)(2,1)} %collective-permute-done.gate2_ref, ...), custom_call_target="tpu_custom_call" | custom-call | flops 30000001024 | bytes 8000000 | tf_op jit(solution)/shard_map/combine/pallas_call | solution.py:416
  214.6 1.7 add_convert_fusion
  (27 shorter events, 0.2 us)
Async XLA Ops:
  6.5 1.8 copy-start
  6.6 67.8 %copy-start.6 = (s32[40,4]{0,1:T(4,128)S(1)}, s32[40,4]{0,1:T(4,128)}, u32[]{:S(2)}) copy-start(s32[40,4]{0,1:T(4,128)} %param.28) | copy-start | bytes 1924
  6.6 67.1 %copy-start.8 = (f32[40,4]{0,1:T(4,128)S(1)}, f32[40,4]{0,1:T(4,128)}, u32[]{:S(2)}) copy-start(f32[40,4]{0,1:T(4,128)} %param.29) | copy-start | bytes 1924
  6.6 92.2 %all-gather.2.cloned.1.call-start = ((), (), s32[]{:S(2)}) async-start(), calls=%async_computation.1 | async-start | bytes 5406720 | tf_op jit(solution)/shard_map/all_gather | solution.py:32
  11.5 153.1 %collective-permute-start = (bf16[2048,256]{1,0:T(8,128)(2,1)}, bf16[2048,256]{1,0:T(8,128)(2,1)}, u32[]{:S(2)}, u32[]{:S(2)}) collective-permute-start(bf16[2048,256]{1,0:T(8,128)(2,1)} %bitcast.71), channel_id=1, source_target_pairs={{0,1},{1,0},{2,3},{3,2},{4,5},{5,4},{6,7},{7,6},{8,9},{9,8},{10,11... | collective-permute-start | bytes 3145736 | tf_op jit(solution)/shard_map/ppermute | solution.py:486
  13.3 151.4 %collective-permute-start.1 = (bf16[2048,256]{1,0:T(8,128)(2,1)}, bf16[2048,256]{1,0:T(8,128)(2,1)}, u32[]{:S(2)}, u32[]{:S(2)}) collective-permute-start(bf16[2048,256]{1,0:T(8,128)(2,1)} %bitcast.73), channel_id=1, source_target_pairs={{0,1},{1,0},{2,3},{3,2},{4,5},{5,4},{6,7},{7,6},{8,9},{9,8},{10,11... | collective-permute-start | bytes 3145736 | tf_op jit(solution)/shard_map/ppermute | solution.py:486
  13.7 151.0 %collective-permute-start.2 = (bf16[256,2048]{1,0:T(8,128)(2,1)}, bf16[256,2048]{1,0:T(8,128)(2,1)}, u32[]{:S(2)}, u32[]{:S(2)}) collective-permute-start(bf16[256,2048]{1,0:T(8,128)(2,1)} %bitcast.75), channel_id=1, source_target_pairs={{0,1},{1,0},{2,3},{3,2},{4,5},{5,4},{6,7},{7,6},{8,9},{9,8},{10,11... | collective-permute-start | bytes 3145736 | tf_op jit(solution)/shard_map/ppermute | solution.py:486
  73.6 1.6 copy-start.3
  98.7 3.8 %slice-start = ((s8[5242880]{0:T(1024)(128)(4,1)}), s8[4194304]{0:T(1024)(128)(4,1)S(1)}, s32[]{:S(2)}) async-start(s8[5242880]{0:T(1024)(128)(4,1)} %bitcast.64), calls=%async_computation.2 | async-start | bytes 8388608
  98.7 3.9 %slice-start.1 = ((s8[5242880]{0:T(1024)(128)(4,1)}), s8[1048576]{0:T(1024)(128)(4,1)S(1)}, s32[]{:S(2)}) async-start(s8[5242880]{0:T(1024)(128)(4,1)} %bitcast.64), calls=%async_computation.3 | async-start | bytes 2097152
  102.0 1.1 copy-start.4
  105.1 6.0 %copy-start.7 = (bf16[40,4]{0,1:T(4,128)(2,1)S(1)}, bf16[40,4]{0,1:T(4,128)(2,1)}, u32[]{:S(2)}) copy-start(bf16[40,4]{0,1:T(4,128)(2,1)} %get-tuple-element.10) | copy-start | bytes 964
  105.1 11.8 %copy-start.5 = (bf16[40,2048]{1,0:T(8,128)(2,1)S(1)}, bf16[40,2048]{1,0:T(8,128)(2,1)}, u32[]{:S(2)}) copy-start(bf16[40,2048]{1,0:T(8,128)(2,1)} %param.22) | copy-start | bytes 491524
  106.7 10.1 %all-to-all-start = ((bf16[4,40,256]{2,1,0:T(8,128)(2,1)}), bf16[4,40,256]{2,1,0:T(8,128)(2,1)S(1)}, u32[]{:S(2)}, u32[]{:S(2)}) async-start(bf16[4,40,256]{2,1,0:T(8,128)(2,1)} %all_to_all.14), calls=%async_computation | async-start | bytes 163840 | tf_op jit(solution)/shard_map/all_to_all | solution.py:537
  162.7 1.3 copy-start.1
  164.0 0.6 copy-start.2
Sparse Core Ops, SparseCore 0:
  11.6 87.0 all-gather.1

commit v2 on v1

--- a/solution.py
+++ b/solution.py
@@ -25,15 +25,6 @@
 SLOTS = 8
 HALF = 64
 SPLIT = 2
-
-
-def sent_together(arrays, axis, dim, along):
-    both = jnp.concatenate(arrays, axis=along)
-    result, at, finished = (lax.all_gather(both, axis, axis=dim, tiled=True), 0, [])
-    for a in arrays:
-        finished.append(lax.slice_in_dim(result, at, at + a.shape[along], axis=along))
-        at += a.shape[along]
-    return tuple(finished)
 
 
 def turn(vector, row_shift, col_shift):
@@ -59,15 +50,6 @@
             )
         )
     return jnp.concatenate(pieces, axis=-1)
-
-
-def norm_scale(values, gain):
-    wide = values.astype(jnp.float32)
-    return (
-        wide
-        * lax.rsqrt(jnp.mean(wide * wide, axis=-1, keepdims=True) + eps)
-        * gain.astype(jnp.float32)
-    )
 
 
 def greet(peers):
@@ -446,6 +428,270 @@
     )(sent, notes, *weights)
 
 
+def attention_kernel(
+    latent_ref,
+    gain_ref,
+    key_w_ref,
+    value_w_ref,
+    pairs_ref,
+    query_ref,
+    residual_ref,
+    ffn_gain_ref,
+    out_w_ref,
+    hidden_ref,
+    normed_ref,
+    store,
+    rots,
+    summed,
+    peaks,
+    totals,
+    staged,
+    heads,
+    out_w,
+    out_w_sem,
+    ring_send,
+    ring_recv,
+    rot_send,
+    rot_recv,
+    side_send,
+    side_recv,
+    side_rot_send,
+    side_rot_recv,
+    tp_send,
+    tp_recv,
+):
+    z, c, ring, near = places()
+    x = lax.axis_index("tp")
+    tp = lax.axis_size("tp")
+    steps = store.shape[0]
+    tokens = latent_ref.shape[0]
+    heads_dev = query_ref.shape[0]
+    key_width = key_w_ref.shape[1]
+    rows = residual_ref.shape[0]
+    piece = tokens // SPLIT
+    last = (steps - 1, steps - 2)
+    load = pltpu.make_async_copy(out_w_ref, out_w, out_w_sem)
+    load.start()
+    wide = latent_ref[...].astype(jnp.float32)
+    wide = (
+        wide
+        * lax.rsqrt(jnp.mean(wide * wide, axis=-1, keepdims=True) + eps)
+        * gain_ref[...].astype(jnp.float32)
+    ).astype(jnp.bfloat16)
+    own = slice(2 * tokens, 3 * tokens)
+    store[steps - 1, own, 0:key_width] = jnp.dot(
+        wide, key_w_ref[...], preferred_element_type=jnp.float32
+    ).astype(jnp.bfloat16)
+    store[steps - 1, own, key_width:] = jnp.dot(
+        wide, value_w_ref[...], preferred_element_type=jnp.float32
+    ).astype(jnp.bfloat16)
+    rots[steps - 1, 2] = pairs_ref[...]
+    summed[...] = jnp.zeros_like(summed)
+    totals[...] = jnp.zeros_like(totals)
+    peaks[...] = jnp.full_like(peaks, -jnp.inf)
+    others = [{"tp": lax.rem(x + r, tp)} for r in range(1, tp)]
+    greet((*ring, near[0], *others))
+
+    def ring_copy(d, j, h):
+        source = (
+            store.at[steps - 1, pl.ds(2 * tokens + h * piece, piece)]
+            if j == 0
+            else store.at[j - 1, pl.ds(2 * d * tokens + h * piece, piece)]
+        )
+        return pltpu.make_async_remote_copy(
+            src_ref=source,
+            dst_ref=store.at[j, pl.ds(2 * d * tokens + h * piece, piece)],
+            send_sem=ring_send.at[d, j, h],
+            recv_sem=ring_recv.at[d, j, h],
+            device_id=ring[d],
+            device_id_type=MESH,
+        )
+
+    def rot_copy(d, j):
+        return pltpu.make_async_remote_copy(
+            src_ref=pairs_ref if j == 0 else rots.at[j - 1, 2 * d],
+            dst_ref=rots.at[j, 2 * d],
+            send_sem=rot_send.at[d, j],
+            recv_sem=rot_recv.at[d, j],
+            device_id=ring[d],
+            device_id_type=MESH,
+        )
+
+    def side_copy(d, j):
+        return pltpu.make_async_remote_copy(
+            src_ref=store.at[j, pl.ds(2 * d * tokens, tokens)],
+            dst_ref=store.at[j, pl.ds((2 * d + 1) * tokens, tokens)],
+            send_sem=side_send.at[d, j],
+            recv_sem=side_recv.at[d, j],
+            device_id=near[0],
+            device_id_type=MESH,
+        )
+
+    def side_rot_copy(d, j):
+        return pltpu.make_async_remote_copy(
+            src_ref=rots.at[j, 2 * d],
+            dst_ref=rots.at[j, 2 * d + 1],
+            send_sem=side_rot_send.at[d, j],
+            recv_sem=side_rot_recv.at[d, j],
+            device_id=near[0],
+            device_id_type=MESH,
+        )
+
+    def tp_copy(r):
+        return pltpu.make_async_remote_copy(
+            src_ref=staged.at[lax.rem(x + r, tp)],
+            dst_ref=heads.at[x],
+            send_sem=tp_send.at[r - 1],
+            recv_sem=tp_recv.at[r - 1],
+            device_id=others[r - 1],
+            device_id_type=MESH,
+        )
+
+    factor = (PLAIN_HEAD_WIDTH + QK_ROPE) ** (-0.5) * 1.4426950408889634
+
+    def attend(j):
+        for d in range(2):
+            side_copy(d, j).wait_recv()
+            side_rot_copy(d, j).wait_recv()
+        turned = []
+        for b in range(4):
+            pair = rots[j, b]
+            turned.append(pair)
+            turned.append(jnp.concatenate([pair[:, QK_ROPE:], pair[:, :QK_ROPE]], axis=1))
+        turned = jnp.concatenate(turned, axis=0)
+        for head in range(heads_dev):
+            at = head * PLAIN_HEAD_WIDTH
+            keys = jnp.concatenate([store[j, :, at : at + PLAIN_HEAD_WIDTH], turned], axis=1)
+            scores = lax.dot_general(
+                query_ref[head],
+                keys,
+                (((1,), (1,)), ((), ())),
+                preferred_element_type=jnp.float32,
+            )
+            before = peaks[head]
+            peak = jnp.maximum(before, jnp.max(scores, axis=1, keepdims=True))
+            weights = jnp.exp2((scores - peak[:, 0:1]) * factor)
+            keep = jnp.exp2((before - peak) * factor)
+            totals[head] = totals[head] * keep + jnp.sum(weights, axis=1, keepdims=True)
+            at = key_width + head * VALUE_WIDTH
+            summed[head] = summed[head] * keep + jnp.dot(
+                weights.astype(jnp.bfloat16),
+                store[j, :, at : at + VALUE_WIDTH],
+                preferred_element_type=jnp.float32,
+            )
+            peaks[head] = peak
+
+    for h in range(SPLIT):
+        for d in range(2):
+            ring_copy(d, 0, h).start()
+            if h == 0:
+                rot_copy(d, 0).start()
+    side_copy(1, steps - 1).start()
+    side_rot_copy(1, steps - 1).start()
+    for j in range(steps):
+        for h in range(SPLIT):
+            for d in range(2):
+                if j <= last[d]:
+                    ring_copy(d, j, h).wait_recv()
+                    if j < last[d]:
+                        ring_copy(d, j + 1, h).start()
+                    if h == 0:
+                        rot_copy(d, j).wait_recv()
+                        if j < last[d]:
+                            rot_copy(d, j + 1).start()
+        for d in range(2):
+            if j <= last[d]:
+                side_copy(d, j).start()
+                side_rot_copy(d, j).start()
+        if j > 0:
+            attend(j - 1)
+    attend(steps - 1)
+    done = jnp.concatenate(
+        [summed[head] / totals[head] for head in range(heads_dev)], axis=1
+    )
+    for t in range(tp):
+        staged[t] = done[t * rows : (t + 1) * rows].astype(jnp.bfloat16)
+    for r in range(1, tp):
+        tp_copy(r).start()
+    heads[x] = staged[x]
+    load.wait()
+    for r in range(1, tp):
+        tp_copy(r).wait_recv()
+    total = residual_ref[...].astype(jnp.float32)
+    width = heads.shape[2]
+    for t in range(tp):
+        total = total + jnp.dot(
+            heads[t], out_w[t * width : (t + 1) * width], preferred_element_type=jnp.float32
+        )
+    hidden = total.astype(jnp.bfloat16)
+    hidden_ref[...] = hidden
+    wide = hidden.astype(jnp.float32)
+    normed_ref[...] = (
+        wide
+        * lax.rsqrt(jnp.mean(wide * wide, axis=-1, keepdims=True) + eps)
+        * ffn_gain_ref[...].astype(jnp.float32)
+    ).astype(jnp.bfloat16)
+    for r in range(1, tp):
+        tp_copy(r).wait_send()
+    for j in range(steps):
+        for d in range(2):
+            if j <= last[d]:
+                rot_copy(d, j).wait_send()
+                for h in range(SPLIT):
+                    ring_copy(d, j, h).wait_send()
+            side_copy(d, j).wait_send()
+            side_rot_copy(d, j).wait_send()
+
+
+def attention(
+    latent, gain, key_w, value_w, pairs, query, residual, ffn_gain, out_w, steps, tp
+):
+    tokens = latent.shape[0]
+    rows, width = residual.shape
+    heads_dev = query.shape[0]
+    store_width = key_w.shape[1] + value_w.shape[1]
+    vmem = pl.BlockSpec(memory_space=pltpu.VMEM)
+    bf16 = jnp.bfloat16
+    dma = pltpu.SemaphoreType.DMA
+    return pl.pallas_call(
+        attention_kernel,
+        name="attention",
+        out_shape=(
+            jax.ShapeDtypeStruct((rows, width), bf16),
+            jax.ShapeDtypeStruct((rows, width), bf16),
+        ),
+        in_specs=[vmem] * 8 + [pl.BlockSpec(memory_space=pl.ANY)],
+        out_specs=(vmem, vmem),
+        scratch_shapes=[
+            pltpu.VMEM((steps, 4 * tokens, store_width), bf16),
+            pltpu.VMEM((steps, 4, *pairs.shape), bf16),
+            pltpu.VMEM((heads_dev, tokens, VALUE_WIDTH), jnp.float32),
+            pltpu.VMEM((heads_dev, tokens, VALUE_WIDTH), jnp.float32),
+            pltpu.VMEM((heads_dev, tokens, VALUE_WIDTH), jnp.float32),
+            pltpu.VMEM((tp, rows, heads_dev * VALUE_WIDTH), bf16),
+            pltpu.VMEM((tp, rows, heads_dev * VALUE_WIDTH), bf16),
+            pltpu.VMEM(out_w.shape, bf16),
+            dma,
+            dma((2, steps, SPLIT)),
+            dma((2, steps, SPLIT)),
+            dma((2, steps)),
+            dma((2, steps)),
+            dma((2, steps)),
+            dma((2, steps)),
+            dma((2, steps)),
+            dma((2, steps)),
+            dma((tp - 1,)),
+            dma((tp - 1,)),
+        ],
+        compiler_params=pltpu.CompilerParams(
+            collective_id=3, has_side_effects=True, vmem_limit_bytes=40 * 2**20
+        ),
+        cost_estimate=pl.CostEstimate(
+            flops=30_000_000_000, bytes_accessed=8_000_000, transcendentals=0
+        ),
+    )(latent, gain, key_w, value_w, pairs, query, residual, ffn_gain, out_w)
+
+
 def routing_note(routes, route_weights, experts):
     rows, top = routes.shape
     flat = routes.reshape(rows * top)
@@ -489,56 +735,31 @@
     place = lax.axis_index(SP) * tok_dev + jnp.arange(tok_dev, dtype=jnp.int32)
     grid_row = place // GRID_W
     grid_col = place % GRID_W
-    normed_latent = norm_scale(latent, latent_norm_scale).astype(jnp.bfloat16)
-    key_plain = jnp.dot(normed_latent, plain_key_matrix, preferred_element_type=jnp.float32).astype(
-        jnp.bfloat16
-    )
-    values = jnp.dot(normed_latent, value_matrix, preferred_element_type=jnp.float32).astype(
-        jnp.bfloat16
-    )
     key_rot = turn(key_turn.astype(jnp.float32), grid_row, grid_col).astype(jnp.bfloat16)
-    key_pairs = key_rot.reshape(tok_dev // 2, 2 * QK_ROPE)
+    key_pairs = jnp.concatenate([key_rot[: tok_dev // 2], key_rot[tok_dev // 2 :]], axis=1)
     query_rot = turn(
         query_turn.astype(jnp.float32).reshape(tok_dev, heads_dev, QK_ROPE), grid_row, grid_col
     ).astype(jnp.bfloat16)
     plain_query = query_plain.reshape(tok_dev, heads_dev, PLAIN_HEAD_WIDTH)
-    scale = (PLAIN_HEAD_WIDTH + QK_ROPE) ** (-0.5)
-    piece_keys, piece_values, piece_pairs = (
-        *sent_together((key_plain, values), SP, 0, 1),
-        lax.all_gather(key_pairs, SP, axis=0, tiled=True),
+    query = jnp.concatenate(
+        [plain_query, query_rot, jnp.zeros_like(query_rot)], axis=2
+    ).transpose(1, 0, 2)
+    rows_dev = residual.shape[0]
+    steps = lax.axis_size("sp_0") // 2
+    hidden, normed = attention(
+        latent,
+        latent_norm_scale[None],
+        plain_key_matrix,
+        value_matrix,
+        key_pairs,
+        query,
+        residual,
+        ffn_gain[None],
+        out_weight,
+        steps,
+        tp,
     )
-    count = piece_keys.shape[0]
-    piece_rot = piece_pairs.reshape(count, QK_ROPE)
-    new_total = []
-    new_summed = []
-    for head in range(heads_dev):
-        head_keys = piece_keys[:, head * PLAIN_HEAD_WIDTH : (head + 1) * PLAIN_HEAD_WIDTH]
-        head_values = piece_values[:, head * VALUE_WIDTH : (head + 1) * VALUE_WIDTH]
-        scores = (
-            jnp.einsum(
-                "qd,kd->qk", plain_query[:, head], head_keys, preferred_element_type=jnp.float32
-            )
-            + jnp.einsum(
-                "qd,kd->qk", query_rot[:, head], piece_rot, preferred_element_type=jnp.float32
-            )
-        ) * scale
-        peak = jnp.max(scores, axis=1)
-        weights = jnp.exp(scores - peak[:, None])
-        new_total.append(jnp.sum(weights, axis=1))
-        new_summed.append(
-            jnp.dot(weights.astype(jnp.bfloat16), head_values, preferred_element_type=jnp.float32)
-        )
-    total = jnp.stack(new_total)
-    summed = jnp.stack(new_summed)
-    attended = jnp.transpose((summed / total[..., None]).astype(jnp.bfloat16), (1, 0, 2)).reshape(
-        tok_dev, heads_dev * VALUE_WIDTH
-    )
-    rows_dev = residual.shape[0]
-    token_heads = lax.all_to_all(attended, "tp", split_axis=0, concat_axis=1, tiled=True)
-    projected = jnp.dot(token_heads, out_weight, preferred_element_type=jnp.float32)
-    hidden = (residual.astype(jnp.float32) + projected).astype(jnp.bfloat16)
-    normed = norm_scale(hidden, ffn_gain).astype(jnp.bfloat16)
-    sent, notes = dispatch(normed, note, lax.axis_size("sp_0") // 2)
+    sent, notes = dispatch(normed, note, steps)
     mixed = combine(sent, notes, (*own_weights, *other_weights), rows_dev)
     return (hidden.astype(jnp.float32) + mixed).astype(jnp.bfloat16)
 

time: 224 us -> 193 us (0.86)
  Pallas kernels: 92.4 us -> 174 us
  blocking collectives: 52 us -> 0 us
  waiting for transfers between devices: 25 us -> 0.01 us
  matrix products: 15.2 us -> 0 us
  between operations: 13.7 us -> 0.28 us
  starting transfers between devices: 8.17 us -> 3.78 us
  other arithmetic: 8.8 us -> 4.93 us
  local copies, waits for them, and re-layouts: 7.75 us -> 10.1 us
    pallas_call x0 -> x1, Pallas kernels: none -> 67.9 us  [attention(): pl.pallas_call(attention_kernel, name='attention', out_shape=(jax.ShapeDt...]
    all_gather x1 -> x0, blocking collectives: 52 us -> none  [on_device(): lax.all_gather(key_pairs, SP, axis=0, tiled=True)]
    all_gather x1 -> x0, waiting for transfers between devices: 19.3 us -> none  [sent_together(): lax.all_gather(both, axis, axis=dim, tiled=True)]
    dot_general x9 -> x0, matrix products: 15.2 us -> none  [the longest x2 4.27 us: on_device(): jnp.einsum('qd,kd->qk', query_rot[:, head], piece_rot, preferred_element_...]
    pallas_call x1, Pallas kernels: 42.6 us -> 55.9 us  [dispatch(): pl.pallas_call(dispatch_kernel, name='dispatch', out_shape=(jax.ShapeDtyp...]
    all_to_all x1 -> x0, waiting for transfers between devices: 5.68 us -> none  [on_device(): lax.all_to_all(attended, 'tp', split_axis=0, concat_axis=1, tiled=True)]
    all_to_all x1 -> x0, starting transfers between devices: 4.39 us -> none  [on_device(): lax.all_to_all(attended, 'tp', split_axis=0, concat_axis=1, tiled=True)]
    unnamed x24 -> x25, local copies, waits for them, and re-layouts: 4.11 us -> 8.05 us
  transfers between devices with their start and end apart: 5 -> 3, of which waited for: 2 -> 0; matrix products, arithmetic and copies ran while one was open for 10% -> 4% of each run, Pallas kernels for 19% -> 64%
where the time goes in v2:
time: 193 us
  Pallas kernels  174 us (90%)
  local copies, waits for them, and re-layouts  10.1 us (5%)
  other arithmetic  4.93 us (3%)
  starting transfers between devices  3.78 us (2%)
    pallas_call x1, Pallas kernels, attention(): pl.pallas_call(attention_kernel, name='attention', out_shape=(jax.ShapeDt...  67.9 us
    pallas_call x1, Pallas kernels, dispatch(): pl.pallas_call(dispatch_kernel, name='dispatch', out_shape=(jax.ShapeDtyp...  55.9 us
    pallas_call x1, Pallas kernels, combine(): pl.pallas_call(combine_kernel, name='combine', out_shape=jax.ShapeDtypeSt...  49.9 us
    unnamed x25, local copies, waits for them, and re-layouts  8.05 us
  transfers between devices with their start and end apart: 3, of which 0 were waited for; matrix products, arithmetic and copies ran while one was open for 4% of the time, Pallas kernels for 64%

profile of v2, /device:TPU:40, one launch (start us, length us, event | category | flops | bytes accessed | tf_op | source)
XLA Modules:
  0.0 192.8 jit_solution(4477846038266096341)
XLA Ops:
  0.0 0.0 copy-start
  0.0 0.0 copy-start.5
  0.0 0.0 copy-start.3
  0.0 0.0 copy-start.2
  0.0 0.0 copy-start.4
  0.0 1.7 collective-permute-start
  1.8 0.4 collective-permute-start.1
  2.2 1.6 collective-permute-start.2
  3.8 0.7 broadcast_in_dim.6.gain_ref
  4.5 0.8 subtract_convert_fusion.4
  5.3 0.7 broadcast_in_dim.8.ffn_gain_ref
  6.0 0.8 copy.37
  6.7 0.1 eq.24
  6.9 0.6 reduce-window.6
  7.5 0.2 slice_reduce_fusion
  7.7 0.1 bitcast_bitcast_fusion
  7.8 0.1 reduce_sum.12
  7.9 0.1 copy.40
  8.0 0.7 add_convert_fusion.5
  8.7 0.9 copy.28
  9.6 0.9 copy.31
  10.5 0.0 copy-done
  10.5 0.1 copy.43
  10.6 0.1 copy.44
  10.7 0.1 copy.41
  10.8 0.1 copy.42
  11.0 0.7 multiply_cosine_fusion.1
  11.7 0.1 pad_maximum_fusion
  11.8 0.1 pad_maximum_fusion.1.pairs_ref
  12.0 0.2 concatenate.18
  12.2 0.0 copy-done.5
  12.3 0.0 copy-done.3
  12.3 0.0 copy-done.2
  12.3 0.0 copy-done.4
  12.3 0.0 copy-start.1
  12.3 2.2 %copy-done.1 = bf16[1024,2048]{1,0:T(8,128)(2,1)S(1)} copy-done((bf16[1024,2048]{1,0:T(8,128)(2,1)S(1)}, bf16[1024,2048]{1,0:T(8,128)(2,1)}, u32[]{:S(2)}) %copy-start.1) | copy-done | bytes 4194328
  14.5 67.9 %attention.1 = (bf16[40,2048]{1,0:T(8,128)(2,1)S(1)}, bf16[40,2048]{1,0:T(8,128)(2,1)S(1)}) custom-call(bf16[160,512]{1,0:T(8,128)(2,1)S(1)} %copy-done.4, bf16[1,512]{1,0:T(2,128)(2,1)S(1)} %broadcast_in_dim.6.gain_ref, bf16[512,256]{1,0:T(8,128)(2,1)S(1)} %copy-done.2, bf16[512,256]{1,0:T(8,128)(2,1)S(1)} %copy-done.3, ...), custom_call_target="tpu_custom_call" | custom-call | flops 30000001024 | bytes 8000000 | tf_op jit(solution)/shard_map/attention/pallas_call | solution.py:656
  82.4 55.9 %dispatch.1 = (bf16[8,64,2048]{2,1,0:T(8,128)(2,1)S(1)}, f32[8,16,128]{2,1,0:T(8,128)S(1)}) custom-call(bf16[40,2048]{1,0:T(8,128)(2,1)S(1)} %get-tuple-element.10.norm_ref, bf16[16,128]{1,0:T(8,128)(2,1)S(1)} %pad.9.note_ref), custom_call_target="tpu_custom_call" | custom-call | flops 30000001024 | bytes 8000000 | tf_op jit(solution)/shard_map/dispatch/pallas_call | solution.py:202
  138.3 0.0 copy-start.6
  138.3 1.3 copy-done.6
  139.7 0.0 copy-start.7
  139.7 0.6 copy-done.7
  140.3 0.0 collective-permute-done.gate2_ref
  140.3 0.0 copy-start.8
  140.3 0.0 collective-permute-done.1.up2_ref
  140.3 0.0 collective-permute-done.2.down2_ref
  140.3 1.0 copy-done.8
  141.3 49.9 %combine.1 = f32[40,2048]{1,0:T(8,128)} custom-call(bf16[8,64,2048]{2,1,0:T(8,128)(2,1)} %copy-done.6, f32[8,16,128]{2,1,0:T(8,128)} %copy-done.7, bf16[2048,256]{1,0:T(8,128)(2,1)} %bitcast.28, bf16[2048,256]{1,0:T(8,128)(2,1)} %bitcast.30, bf16[256,2048]{1,0:T(8,128)(2,1)} %bitcast.32, bf16[2048,256]{1,0:T(8,128)(2,1)} %copy-done.8, ...), custom_call_target="tpu_custom_call" | custom-call | flops 30000001024 | bytes 8000000 | tf_op jit(solution)/shard_map/combine/pallas_call | solution.py:398
  191.2 1.7 add_convert_fusion
  (16 shorter events, 0.3 us)
Async XLA Ops:
  0.0 10.5 %copy-start = (bf16[160,256]{1,0:T(8,128)(2,1)S(1)}, bf16[160,256]{1,0:T(8,128)(2,1)}, u32[]{:S(2)}) copy-start(bf16[160,256]{1,0:T(8,128)(2,1)} %param.15) | copy-start | bytes 245764
  0.0 12.2 %copy-start.5 = (bf16[40,2048]{1,0:T(8,128)(2,1)S(1)}, bf16[40,2048]{1,0:T(8,128)(2,1)}, u32[]{:S(2)}) copy-start(bf16[40,2048]{1,0:T(8,128)(2,1)} %residual_ref.1) | copy-start | bytes 491524
  0.0 12.3 %copy-start.3 = (bf16[512,256]{1,0:T(8,128)(2,1)S(1)}, bf16[512,256]{1,0:T(8,128)(2,1)}, u32[]{:S(2)}) copy-start(bf16[512,256]{1,0:T(8,128)(2,1)} %value_w_ref.1) | copy-start | bytes 786436
  0.0 12.3 %copy-start.2 = (bf16[512,256]{1,0:T(8,128)(2,1)S(1)}, bf16[512,256]{1,0:T(8,128)(2,1)}, u32[]{:S(2)}) copy-start(bf16[512,256]{1,0:T(8,128)(2,1)} %key_w_ref.1) | copy-start | bytes 786436
  0.0 12.3 %copy-start.4 = (bf16[160,512]{1,0:T(8,128)(2,1)S(1)}, bf16[160,512]{1,0:T(8,128)(2,1)}, u32[]{:S(2)}) copy-start(bf16[160,512]{1,0:T(8,128)(2,1)} %latent_ref.1) | copy-start | bytes 491524
  0.0 140.3 %collective-permute-start = (bf16[2048,256]{1,0:T(8,128)(2,1)}, bf16[2048,256]{1,0:T(8,128)(2,1)S(1)}, u32[]{:S(2)}, u32[]{:S(2)}) collective-permute-start(bf16[2048,256]{1,0:T(8,128)(2,1)} %bitcast.27), channel_id=1, source_target_pairs={{0,1},{1,0},{2,3},{3,2},{4,5},{5,4},{6,7},{7,6},{8,9},{9,8},{10,11... | collective-permute-start | bytes 3145736 | tf_op jit(solution)/shard_map/ppermute | solution.py:732
  1.8 138.5 %collective-permute-start.1 = (bf16[2048,256]{1,0:T(8,128)(2,1)}, bf16[2048,256]{1,0:T(8,128)(2,1)}, u32[]{:S(2)}, u32[]{:S(2)}) collective-permute-start(bf16[2048,256]{1,0:T(8,128)(2,1)} %bitcast.29), channel_id=1, source_target_pairs={{0,1},{1,0},{2,3},{3,2},{4,5},{5,4},{6,7},{7,6},{8,9},{9,8},{10,11... | collective-permute-start | bytes 3145736 | tf_op jit(solution)/shard_map/ppermute | solution.py:732
  2.2 138.1 %collective-permute-start.2 = (bf16[256,2048]{1,0:T(8,128)(2,1)}, bf16[256,2048]{1,0:T(8,128)(2,1)}, u32[]{:S(2)}, u32[]{:S(2)}) collective-permute-start(bf16[256,2048]{1,0:T(8,128)(2,1)} %bitcast.31), channel_id=1, source_target_pairs={{0,1},{1,0},{2,3},{3,2},{4,5},{5,4},{6,7},{7,6},{8,9},{9,8},{10,11... | collective-permute-start | bytes 3145736 | tf_op jit(solution)/shard_map/ppermute | solution.py:732
  12.3 2.2 %copy-start.1 = (bf16[1024,2048]{1,0:T(8,128)(2,1)S(1)}, bf16[1024,2048]{1,0:T(8,128)(2,1)}, u32[]{:S(2)}) copy-start(bf16[1024,2048]{1,0:T(8,128)(2,1)} %out_w_ref.1) | copy-start | bytes 12582916
  138.3 1.3 copy-start.6
  139.7 0.6 copy-start.7
  140.3 1.0 copy-start.8

commit v3 on v0

v3 whole, which is shorter than its diff:
```python
import math

import jax
import jax.numpy as jnp
from jax import lax
from jax.experimental import pallas as pl
from jax.experimental.pallas import tpu as pltpu
from jax.sharding import Mesh
from jax.sharding import PartitionSpec as P

PLAIN_HEAD_WIDTH = 128
QK_ROPE = 64
VALUE_WIDTH = 128
GRID_W = 64
SP = ("sp_0", "sp_1")
GRP_SP = ("grp", "sp_0", "sp_1")
GRP_SP_TP = ("grp", "sp_0", "sp_1", "tp")
MESH = pl.DeviceIdType.MESH

theta = 10000.0
eps = 1e-06
limit = 7.0
slope = 1.702

SLOTS = 8
HALF = 64
SPLIT = 2
CHUNKS = 8


def matches(z, c, target):
    row = lax.broadcasted_iota(jnp.int32, (4 * SLOTS, 2 * HALF), 0)
    lane = lax.broadcasted_iota(jnp.int32, (4 * SLOTS, 2 * HALF), 1)
    core = jnp.where(row < 2 * SLOTS, c, 1 - c)
    wanted = ((2 * z + core) * SLOTS + row % SLOTS).astype(jnp.float32)
    same = (row // SLOTS) % 2 == lane // HALF
    return [
        jnp.logical_and(same, jnp.broadcast_to(target[k : k + 1], wanted.shape) == wanted)
        for k in range(4)
    ]


def layer_kernel(
    latent_hbm,
    gain_ref,
    key_w_hbm,
    value_w_hbm,
    key_turn_ref,
    query_hbm,
    query_turn_hbm,
    residual_hbm,
    ffn_gain_ref,
    routes_ref,
    route_weights_ref,
    out_w_hbm,
    gate_hbm,
    up_hbm,
    down_hbm,
    out_ref,
    latent_ref,
    key_w_ref,
    value_w_ref,
    query_ref,
    query_turn_ref,
    residual_ref,
    out_w,
    query,
    store,
    rots,
    summed,
    peaks,
    totals,
    staged,
    heads,
    hidden_ref,
    notes,
    padded,
    blocks,
    chosen,
    taken,
    gate_w,
    up_w,
    down_w,
    product,
    back,
    token,
    own_part,
    arrive,
    leave,
    load_sem,
    weight_sem,
    chunk_send,
    chunk_recv,
    key_send,
    key_recv,
    rot_send,
    rot_recv,
    side_send,
    side_recv,
    side_rot_send,
    side_rot_recv,
    note_send,
    note_recv,
    tp_send,
    tp_recv,
    row_send,
    row_recv,
    go_send,
    go_recv,
    come_send,
    come_recv,
    sum_send,
    sum_recv,
):
    z = lax.axis_index("sp_0")
    c = lax.axis_index("sp_1")
    x = lax.axis_index("tp")
    tp = lax.axis_size("tp")
    ring_size = lax.axis_size("sp_0")
    mirror = tp - 1 - x
    mate = x + 1 - 2 * lax.rem(x, 2)
    ring = ({"sp_0": lax.rem(z + 1, ring_size)}, {"sp_0": lax.rem(z + ring_size - 1, ring_size)})
    near = ({"sp_1": 1 - c}, {"tp": mirror}, {"sp_1": 1 - c, "tp": mirror})
    others = [{"tp": lax.rem(x + r, tp)} for r in range(1, tp)]
    steps = store.shape[0]
    end = steps - 1
    tokens = latent_ref.shape[0]
    rows, width = residual_ref.shape
    heads_dev = query.shape[0]
    key_width = key_w_ref.shape[1]
    span = 2 * SLOTS

    loads = [
        pltpu.make_async_copy(source, target, load_sem.at[i])
        for i, (source, target) in enumerate(
            (
                (latent_hbm, latent_ref),
                (key_w_hbm, key_w_ref),
                (value_w_hbm, value_w_ref),
                (query_turn_hbm, query_turn_ref),
                (query_hbm, query_ref),
                (residual_hbm, residual_ref),
                (out_w_hbm, out_w),
            )
        )
    ]
    for load in loads:
        load.start()
    own_weights = [
        pltpu.make_async_copy(source.at[0], target.at[0], weight_sem.at[i])
        for i, (source, target) in enumerate(
            ((gate_hbm, gate_w), (up_hbm, up_w), (down_hbm, down_w))
        )
    ]
    for load in own_weights:
        load.start()

    barrier = pltpu.get_barrier_semaphore()
    greeted = (*ring, near[0], near[2], *others)
    for peer in greeted:
        pl.semaphore_signal(barrier, inc=1, device_id=peer, device_id_type=MESH)

    def remote(source, target, send_sem, recv_sem, device):
        return pltpu.make_async_remote_copy(
            src_ref=source,
            dst_ref=target,
            send_sem=send_sem,
            recv_sem=recv_sem,
            device_id=device,
            device_id_type=MESH,
        )

    def chunk_copy(i):
        kind, at = i // CHUNKS, i % CHUNKS
        source, target = ((gate_hbm, gate_w), (up_hbm, up_w), (down_hbm, down_w))[kind]
        size = source.shape[1] // CHUNKS
        part = pl.ds(at * size, size)
        return remote(
            source.at[0, part],
            target.at[1, part],
            chunk_send.at[i],
            chunk_recv.at[i],
            {"tp": mate},
        )

    issued = []

    def issue_chunks(upto):
        while len(issued) < min(upto, 3 * CHUNKS):
            chunk_copy(len(issued)).start()
            issued.append(None)

    def active(d, j, h):
        return j < end or h * 2 // SPLIT == d

    for j in range(steps):
        for d in range(2):
            blocks[j, d * HALF + rows : (d + 1) * HALF] = jnp.zeros(
                (HALF - rows, width), blocks.dtype
            )
    summed[...] = jnp.zeros_like(summed)
    totals[...] = jnp.zeros_like(totals)
    peaks[...] = jnp.full_like(peaks, -jnp.inf)

    lane = lax.broadcasted_iota(jnp.int32, (tokens, 2 * QK_ROPE), 1)
    place = lax.broadcasted_iota(jnp.int32, (tokens, 2 * QK_ROPE), 0) + (2 * z + c) * tokens
    count = QK_ROPE // 4
    upper = lax.rem(lane // count, 2) == 1
    by_column = lax.rem(lane // (2 * count), 2) == 1
    spot = jnp.where(by_column, lax.rem(place, GRID_W), place // GRID_W).astype(jnp.float32)
    freqs = jnp.exp(lax.rem(lane, count).astype(jnp.float32) * (-math.log(theta) / count))
    angle = spot * freqs
    cosine = jnp.cos(angle)
    sine = jnp.sin(angle)
    sine = jnp.where(upper, sine, -sine)

    def turned(values):
        partner = jnp.where(
            upper, pltpu.roll(values, count, 1), pltpu.roll(values, 2 * QK_ROPE - count, 1)
        )
        return values * cosine + partner * sine

    flat = jnp.transpose(key_turn_ref[...].astype(jnp.float32))
    twice = turned(jnp.concatenate([flat, flat], axis=1))
    left = lane < QK_ROPE
    rots[end, 2] = jnp.where(
        left[: tokens // 2], twice[: tokens // 2], twice[tokens // 2 :]
    ).astype(jnp.bfloat16)

    padded[0] = jnp.full(padded.shape[1:], -1.0, jnp.float32)
    padded[1] = jnp.zeros(padded.shape[1:], jnp.float32)
    top = routes_ref.shape[0]
    padded[0, 0:top, 0:rows] = routes_ref[...].astype(jnp.float32)
    padded[1, 0:top, 0:rows] = route_weights_ref[...]
    experts = 2 * ring_size
    lanes = 2 * HALF
    numbers = lax.broadcasted_iota(jnp.int32, (experts, lanes), 0).astype(jnp.float32)
    marks = [
        (jnp.broadcast_to(padded[0, k : k + 1], numbers.shape) == numbers).astype(jnp.float32)
        for k in range(top)
    ]
    earlier = (
        lax.broadcasted_iota(jnp.int32, (lanes, lanes), 0)
        < lax.broadcasted_iota(jnp.int32, (lanes, lanes), 1)
    ).astype(jnp.bfloat16)
    counts = jnp.dot(
        sum(marks).astype(jnp.bfloat16), earlier, preferred_element_type=jnp.float32
    )
    for k in range(top):
        slot = jnp.sum(marks[k] * counts, axis=0, keepdims=True)
        notes[1, end, k : k + 1] = padded[0, k : k + 1] * SLOTS + slot
        notes[1, end, top + k : top + k + 1] = padded[1, k : k + 1]

    for load in loads[:3]:
        load.wait()
    wide = latent_ref[...].astype(jnp.float32)
    wide = (
        wide
        * lax.rsqrt(jnp.mean(wide * wide, axis=-1, keepdims=True) + eps)
        * gain_ref[...].astype(jnp.float32)
    ).astype(jnp.bfloat16)
    mine = slice(2 * tokens, 3 * tokens)
    store[end, mine, 0:key_width] = jnp.dot(
        wide, key_w_ref[...], preferred_element_type=jnp.float32
    ).astype(jnp.bfloat16)
    store[end, mine, key_width:] = jnp.dot(
        wide, value_w_ref[...], preferred_element_type=jnp.float32
    ).astype(jnp.bfloat16)
    pl.semaphore_wait(barrier, len(greeted))

    piece = tokens // SPLIT

    def key_copy(d, j, h):
        source_step, source_slot = (end, 2) if j == 0 else (j - 1, 2 * d)
        slot = 2 * d if j < end else 0
        return remote(
            store.at[source_step, pl.ds(source_slot * tokens + h * piece, piece)],
            store.at[j, pl.ds(slot * tokens + h * piece, piece)],
            key_send.at[d, j, h],
            key_recv.at[d, j, h],
            ring[d],
        )

    def rot_copy(d, j):
        return remote(
            rots.at[end, 2] if j == 0 else rots.at[j - 1, 2 * d],
            rots.at[j, 2 * d],
            rot_send.at[d, j],
            rot_recv.at[d, j],
            ring[d],
        )

    def note_copy(d, j):
        return remote(
            notes.at[1, end] if j == 0 else notes.at[d, j - 1],
            notes.at[d, j],
            note_send.at[d, j],
            note_recv.at[d, j],
            ring[d],
        )

    def side_copy(d, j):
        return remote(
            store.at[j, pl.ds(2 * d * tokens, tokens)],
            store.at[j, pl.ds((2 * d + 1) * tokens, tokens)],
            side_send.at[d, j],
            side_recv.at[d, j],
            near[0],
        )

    def side_rot_copy(d, j):
        return remote(
            rots.at[j, 2 * d],
            rots.at[j, 2 * d + 1],
            side_rot_send.at[d, j],
            side_rot_recv.at[d, j],
            near[0],
        )

    def tp_copy(r):
        return remote(
            staged.at[lax.rem(x + r, tp)],
            heads.at[x],
            tp_send.at[r - 1],
            tp_recv.at[r - 1],
            others[r - 1],
        )

    factor = (PLAIN_HEAD_WIDTH + QK_ROPE) ** (-0.5) * 1.4426950408889634

    def attend(j):
        for d in range(2):
            side_copy(d, j).wait_recv()
            side_rot_copy(d, j).wait_recv()
        pairs = []
        for b in range(4):
            pair = rots[j, b]
            pairs.append(pair)
            pairs.append(jnp.concatenate([pair[:, QK_ROPE:], pair[:, :QK_ROPE]], axis=1))
        pairs = jnp.concatenate(pairs, axis=0)
        for head in range(heads_dev):
            at = head * PLAIN_HEAD_WIDTH
            keys = jnp.concatenate([store[j, :, at : at + PLAIN_HEAD_WIDTH], pairs], axis=1)
            scores = lax.dot_general(
                query[head],
                keys,
                (((1,), (1,)), ((), ())),
                preferred_element_type=jnp.float32,
            )
            before = peaks[head]
            peak = jnp.maximum(before, jnp.max(scores, axis=1, keepdims=True))
            weights = jnp.exp2((scores - peak[:, 0:1]) * factor)
            keep = jnp.exp2((before - peak) * factor)
            totals[head] = totals[head] * keep + jnp.sum(weights, axis=1, keepdims=True)
            at = key_width + head * VALUE_WIDTH
            summed[head] = summed[head] * keep + jnp.dot(
                weights.astype(jnp.bfloat16),
                store[j, :, at : at + VALUE_WIDTH],
                preferred_element_type=jnp.float32,
            )
            peaks[head] = peak

    for h in range(SPLIT):
        for d in range(2):
            key_copy(d, 0, h).start()
            if h == 0:
                rot_copy(d, 0).start()
    side_copy(1, end).start()
    side_rot_copy(1, end).start()
    for d in range(2):
        note_copy(d, 0).start()
    issue_chunks(2)
    for load in loads[3:5]:
        load.wait()
    spun = turned(query_turn_ref[...].astype(jnp.float32))
    for head in range(heads_dev):
        query[head, :, 0:PLAIN_HEAD_WIDTH] = query_ref[
            :, head * PLAIN_HEAD_WIDTH : (head + 1) * PLAIN_HEAD_WIDTH
        ]
        here = spun if head == 0 else pltpu.roll(spun, 2 * QK_ROPE - head * QK_ROPE, 1)
        query[head, :, PLAIN_HEAD_WIDTH:] = jnp.where(left, here, 0.0).astype(jnp.bfloat16)
    for j in range(steps):
        for h in range(SPLIT):
            for d in range(2):
                if active(d, j, h):
                    key_copy(d, j, h).wait_recv()
                    if j < end and active(d, j + 1, h):
                        key_copy(d, j + 1, h).start()
                if h == 0 and j <= end - d:
                    rot_copy(d, j).wait_recv()
                    if j < end - d:
                        rot_copy(d, j + 1).start()
        for d in range(2):
            if j <= end - d:
                side_copy(d, j).start()
                side_rot_copy(d, j).start()
                note_copy(d, j).wait_recv()
                if j < end - d:
                    note_copy(d, j + 1).start()
        if j < end:
            issue_chunks(2 + (j + 1) * 3 // 2)
        if j > 0:
            attend(j - 1)
    attend(end)
    done = jnp.concatenate([summed[head] / totals[head] for head in range(heads_dev)], axis=1)
    for t in range(tp):
        staged[t] = done[t * rows : (t + 1) * rows].astype(jnp.bfloat16)
    for r in range(1, tp):
        tp_copy(r).start()
    heads[x] = staged[x]
    for load in loads[5:]:
        load.wait()
    for r in range(1, tp):
        tp_copy(r).wait_recv()
    total = residual_ref[...].astype(jnp.float32)
    head_width = heads.shape[2]
    for t in range(tp):
        total = total + jnp.dot(
            heads[t],
            out_w[t * head_width : (t + 1) * head_width],
            preferred_element_type=jnp.float32,
        )
    hidden = total.astype(jnp.bfloat16)
    hidden_ref[...] = hidden
    wide = hidden.astype(jnp.float32)
    blocks[end, HALF : HALF + rows] = (
        wide
        * lax.rsqrt(jnp.mean(wide * wide, axis=-1, keepdims=True) + eps)
        * ffn_gain_ref[...].astype(jnp.float32)
    ).astype(jnp.bfloat16)

    part = width // SPLIT

    def row_copy(d, j, h):
        columns = pl.ds(h * part, part)
        source_step, source_side = (end, 1) if j == 0 else (j - 1, d)
        side = d if j < end else 0
        return remote(
            blocks.at[source_step, pl.ds(source_side * HALF, rows), columns],
            blocks.at[j, pl.ds(side * HALF, rows), columns],
            row_send.at[d, j, h],
            row_recv.at[d, j, h],
            ring[d],
        )

    def go_copy(j, q):
        return remote(
            chosen.at[j, pl.ds((q % 2) * span, span)],
            taken.at[j, pl.ds(q * span, span)],
            go_send.at[j, q - 1],
            go_recv.at[j, q - 1],
            near[q - 1],
        )

    def come_copy(j, q):
        return remote(
            product.at[j, pl.ds(q * span, span)],
            back.at[j, pl.ds(q * span, span)],
            come_send.at[j, q - 1],
            come_recv.at[j, q - 1],
            near[q - 1],
        )

    def sum_copy(d, j, h):
        columns = pl.ds(h * part, part)
        return remote(
            leave.at[d, j, :, columns],
            arrive.at[d, j - 1 if j > 0 else end, :, columns],
            sum_send.at[d, j, h],
            sum_recv.at[d, j, h],
            ring[1 - d],
        )

    def merged(j):
        return jnp.concatenate([notes[0, j][:, :HALF], notes[1, j][:, :HALF]], axis=1)

    for h in range(SPLIT):
        for d in range(2):
            row_copy(d, 0, h).start()
    issue_chunks(15)
    for j in range(steps):
        for h in range(SPLIT):
            for d in range(2):
                if active(d, j, h):
                    row_copy(d, j, h).wait_recv()
                    if j < end and active(d, j + 1, h):
                        row_copy(d, j + 1, h).start()
        picks = sum(m.astype(jnp.float32) for m in matches(z, c, merged(j))).astype(jnp.bfloat16)
        kept = jnp.dot(picks, blocks[j], preferred_element_type=jnp.float32).astype(jnp.bfloat16)
        chosen[j] = kept
        for q in (2, 3, 1):
            go_copy(j, q).start()
        taken[j, 0:span] = kept[0:span]
        issue_chunks(15 + (j + 1) * 3 // 2)
    issue_chunks(3 * CHUNKS)

    group = steps // 2
    for i, (a, b) in enumerate(((group, steps), (0, group))):
        for j in range(a, b):
            for q in (1, 2, 3):
                go_copy(j, q).wait_recv()
        given = taken[a:b].reshape((b - a) * 4 * span, width)
        result = None
        for half in range(2):
            def ready(kind):
                if i == 0 and half == 0:
                    own_weights[kind].wait()
                elif i == 0:
                    for at in range(CHUNKS):
                        chunk_copy(kind * CHUNKS + at).wait_recv()

            ready(0)
            gate = jnp.minimum(
                jnp.dot(given, gate_w[half], preferred_element_type=jnp.float32), limit
            )
            ready(1)
            up = jnp.clip(
                jnp.dot(given, up_w[half], preferred_element_type=jnp.float32), -limit, limit
            )
            act = ((up + 1.0) * gate * jax.nn.sigmoid(slope * gate)).astype(jnp.bfloat16)
            ready(2)
            term = jnp.dot(act, down_w[half], preferred_element_type=jnp.float32)
            result = term if result is None else result + term
        product[a:b] = result.astype(jnp.bfloat16).reshape(b - a, 4 * span, width)
        for j in range(b - 1, a - 1, -1):
            for q in (2, 3, 1):
                come_copy(j, q).start()
            back[j, 0:span] = product[j, 0:span]

    for j in range(end, -1, -1):
        both = merged(j)
        found = matches(z, c, both)
        table = sum(
            jnp.where(m, jnp.broadcast_to(both[top + k : top + k + 1], m.shape), 0.0)
            for k, m in enumerate(found)
        )
        table = jnp.transpose(table)
        table = jnp.concatenate([table, table], axis=1)
        high = table.astype(jnp.bfloat16)
        low = (table - high.astype(jnp.float32)).astype(jnp.bfloat16)
        for q in (1, 2, 3):
            come_copy(j, q).wait_recv()
        token[...] = jnp.dot(high, back[j], preferred_element_type=jnp.float32) + jnp.dot(
            low, back[j], preferred_element_type=jnp.float32
        )
        if j == end:
            own_part[...] = token[HALF : HALF + rows]
        for h in range(SPLIT):
            columns = slice(h * part, (h + 1) * part)
            for d in range(2):
                if not active(d, j, h):
                    continue
                at = d * HALF if j < end else 0
                total = token[at : at + rows, columns]
                if j < end and active(d, j + 1, h):
                    sum_copy(d, j + 1, h).wait_recv()
                    total = total + arrive[d, j, :, columns].astype(jnp.float32)
                leave[d, j, :, columns] = total.astype(jnp.bfloat16)
                sum_copy(d, j, h).start()
    for h in range(SPLIT):
        columns = slice(h * part, (h + 1) * part)
        for d in range(2):
            sum_copy(d, 0, h).wait_recv()
        out_ref[:, columns] = (
            hidden_ref[:, columns].astype(jnp.float32)
            + own_part[:, columns]
            + arrive[0, end, :, columns].astype(jnp.float32)
            + arrive[1, end, :, columns].astype(jnp.float32)
        ).astype(jnp.bfloat16)

    for i in range(3 * CHUNKS):
        chunk_copy(i).wait_send()
    for r in range(1, tp):
        tp_copy(r).wait_send()
    for j in range(steps):
        for d in range(2):
            for h in range(SPLIT):
                if active(d, j, h):
                    key_copy(d, j, h).wait_send()
                    row_copy(d, j, h).wait_send()
                    sum_copy(d, j, h).wait_send()
            if j <= end - d:
                rot_copy(d, j).wait_send()
                note_copy(d, j).wait_send()
            side_copy(d, j).wait_send()
            side_rot_copy(d, j).wait_send()
        for q in (1, 2, 3):
            go_copy(j, q).wait_send()
            come_copy(j, q).wait_send()


def on_device(
    query_plain,
    query_turn,
    latent,
    key_turn,
    latent_norm_scale,
    plain_key_matrix,
    value_matrix,
    residual,
    out_weight,
    ffn_gain,
    gate_weight,
    up_weight,
    down_weight,
    routes,
    route_weights,
):
    tokens = latent.shape[0]
    rows, width = residual.shape
    heads_dev = query_plain.shape[1] // PLAIN_HEAD_WIDTH
    tp = lax.axis_size("tp")
    steps = lax.axis_size("sp_0") // 2
    store_width = plain_key_matrix.shape[1] + value_matrix.shape[1]
    head_width = heads_dev * VALUE_WIDTH
    gate_shape, down_shape = gate_weight.shape[1:], down_weight.shape[1:]
    bf16, f32 = jnp.bfloat16, jnp.float32
    vmem, anywhere = pltpu.VMEM, pl.ANY
    dma = pltpu.SemaphoreType.DMA
    operands = (
        (latent, anywhere),
        (latent_norm_scale.reshape(1, -1), vmem),
        (plain_key_matrix, anywhere),
        (value_matrix, anywhere),
        (key_turn.T, vmem),
        (query_plain, anywhere),
        (query_turn, anywhere),
        (residual, anywhere),
        (ffn_gain.reshape(1, -1), vmem),
        (routes.T, vmem),
        (route_weights.T, vmem),
        (out_weight, anywhere),
        (gate_weight, anywhere),
        (up_weight, anywhere),
        (down_weight, anywhere),
    )
    both_ways = dma((2, steps))
    pieces = dma((2, steps, SPLIT))
    return pl.pallas_call(
        layer_kernel,
        name="layer",
        out_shape=jax.ShapeDtypeStruct((rows, width), bf16),
        in_specs=[pl.BlockSpec(memory_space=space) for _, space in operands],
        out_specs=pl.BlockSpec(memory_space=vmem),
        scratch_shapes=[
            vmem(latent.shape, bf16),
            vmem(plain_key_matrix.shape, bf16),
            vmem(value_matrix.shape, bf16),
            vmem(query_plain.shape, bf16),
            vmem(query_turn.shape, bf16),
            vmem(residual.shape, bf16),
            vmem(out_weight.shape, bf16),
            vmem((heads_dev, tokens, PLAIN_HEAD_WIDTH + 2 * QK_ROPE), bf16),
            vmem((steps, 4 * tokens, store_width), bf16),
            vmem((steps, 4, tokens // 2, 2 * QK_ROPE), bf16),
            vmem((heads_dev, tokens, VALUE_WIDTH), f32),
            vmem((heads_dev, tokens, VALUE_WIDTH), f32),
            vmem((heads_dev, tokens, VALUE_WIDTH), f32),
            vmem((tp, rows, head_width), bf16),
            vmem((tp, rows, head_width), bf16),
            vmem((rows, width), bf16),
            vmem((2, steps, 8, 2 * HALF), f32),
            vmem((2, 8, 2 * HALF), f32),
            vmem((steps, 2 * HALF, width), bf16),
            vmem((steps, 4 * SLOTS, width), bf16),
            vmem((steps, 8 * SLOTS, width), bf16),
            vmem((2, *gate_shape), bf16),
            vmem((2, *gate_shape), bf16),
            vmem((2, *down_shape), bf16),
            vmem((steps, 8 * SLOTS, width), bf16),
            vmem((steps, 8 * SLOTS, width), bf16),
            vmem((2 * HALF, width), f32),
            vmem((rows, width), f32),
            vmem((2, steps, rows, width), bf16),
            vmem((2, steps, rows, width), bf16),
            dma((7,)),
            dma((3,)),
            dma((3 * CHUNKS,)),
            dma((3 * CHUNKS,)),
            pieces,
            pieces,
            both_ways,
            both_ways,
            both_ways,
            both_ways,
            both_ways,
            both_ways,
            both_ways,
            both_ways,
            dma((tp - 1,)),
            dma((tp - 1,)),
            pieces,
            pieces,
            dma((steps, 3)),
            dma((steps, 3)),
            dma((steps, 3)),
            dma((steps, 3)),
            pieces,
            pieces,
        ],
        compiler_params=pltpu.CompilerParams(
            collective_id=1, has_side_effects=True, vmem_limit_bytes=60 * 2**20
        ),
        cost_estimate=pl.CostEstimate(
            flops=30_000_000_000, bytes_accessed=20_000_000, transcendentals=0
        ),
    )(*(array for array, _ in operands))


def solution(mesh):
    torus = Mesh(
        mesh.devices.reshape(mesh.shape["grp"], mesh.shape["sp"] // 2, 2, mesh.shape["tp"]),
        ("grp", "sp_0", "sp_1", "tp"),
    )
    placed = (
        P(GRP_SP, "tp"),
        P(GRP_SP, "tp"),
        P(GRP_SP, None),
        P(GRP_SP, None),
        P(),
        P(None, "tp"),
        P(None, "tp"),
        P(GRP_SP_TP, None),
        P(),
        P(),
        P(SP, None, "tp"),
        P(SP, None, "tp"),
        P(SP, "tp", None),
        P(GRP_SP_TP, None),
        P(GRP_SP_TP, None),
    )
    return jax.shard_map(
        on_device, mesh=torus, in_specs=placed, out_specs=P(GRP_SP_TP, None), check_vma=False
    )
```

time: 312 us -> 161 us (0.52)
  Pallas kernels: 0 us -> 156 us
  blocking collectives: 120 us -> 0 us
  waiting for transfers between devices: 109 us -> 0 us
  matrix products: 29.9 us -> 0 us
  starting transfers between devices: 17 us -> 0 us
  between operations: 13.9 us -> 0.01 us
  other arithmetic: 10.1 us -> 0 us
  local copies, waits for them, and re-layouts: 10.8 us -> 4.12 us
    pallas_call x0 -> x1, Pallas kernels: none -> 156 us  [on_device(): pl.pallas_call(layer_kernel, name='layer', out_shape=jax.ShapeDtypeStruct...]
    all_to_all x2 -> x0, blocking collectives: 67.6 us -> none  [the longest x1 63.1 us: on_device(): lax.all_to_all(outgoing, SP, split_axis=0, concat_axis=0, tiled=True)]
    all_gather x2 -> x0, waiting for transfers between devices: 58.8 us -> none  [the longest x1 37.1 us: turned_gather(): lax.all_gather(both, axis, axis=0, tiled=True)]
    all_gather x1 -> x0, blocking collectives: 52.1 us -> none  [on_device(): lax.all_gather(key_pairs, SP, axis=0, tiled=True)]
    all_to_all x2 -> x0, waiting for transfers between devices: 50 us -> none  [the longest x1 44.4 us: moved_by_axis(): result = lax.all_to_all(result, axes[k], k, k, tiled=True)]
    dot_general x16 -> x0, matrix products: 29.9 us -> none  [the longest x4 6.55 us: expert_whole(): jnp.dot(active[:, index * piece:(index + 1) * piece], down_w[index * piec...]
    all_to_all x2 -> x0, starting transfers between devices: 16.9 us -> none  [the longest x1 12.3 us: moved_by_axis(): result = lax.all_to_all(result, axes[k], k, k, tiled=True)]
    concatenate x4 -> x0, other arithmetic: 3.54 us -> none  [the longest x1 2.83 us: turned_gather(): both = jnp.concatenate([t.reshape(len(t), -1) for t in turned], axis=1)]
  transfers between devices with their start and end apart: 4 -> 0, of which waited for: 4 -> 0; matrix products, arithmetic and copies ran while one was open for 8% -> 0% of each run, Pallas kernels for 0% -> 0%
where the time goes in v3:
time: 161 us; the launch traced here: 160 us
  Pallas kernels  156 us (97%)
  local copies, waits for them, and re-layouts  4.12 us (3%)
    pallas_call x1, Pallas kernels, on_device(): pl.pallas_call(layer_kernel, name='layer', out_shape=jax.ShapeDtypeStruct...  156 us

profile of v3, /device:TPU:40, one launch (start us, length us, event | category | flops | bytes accessed | tf_op | source)
XLA Modules:
  0.0 160.4 jit_solution(8888503311977871876)
XLA Ops:
  0.0 1.2 reshape.6.gain_ref
  1.2 1.3 reshape.7.ffn_gain_ref
  2.5 156.3 %layer.1 = bf16[40,2048]{1,0:T(8,128)(2,1)} custom-call(bf16[160,512]{1,0:T(8,128)(2,1)} %latent_hbm.1, bf16[1,512]{1,0:T(2,128)(2,1)} %reshape.6.gain_ref, bf16[512,256]{1,0:T(8,128)(2,1)} %key_w_hbm.1, bf16[512,256]{1,0:T(8,128)(2,1)} %value_w_hbm.1, bf16[64,160]{1,0:T(8,128)(2,1)} %bitcast.3, bf16[160,256]{1,0:T(8,128)(2,1)} %query_hbm.1, ...), custom_call_target="tpu_custom_call" | custom-call | flops 30000001024 | bytes 20000000 | tf_op jit(solution)/shard_map/layer/pallas_call | solution.py:639
  158.9 1.6 copy.17

commit v4 on v3

--- a/solution.py
+++ b/solution.py
@@ -24,8 +24,9 @@
 
 SLOTS = 8
 HALF = 64
-SPLIT = 2
-CHUNKS = 8
+KEY_SPLIT = 2
+ROW_SPLIT = 4
+CHUNKS = 4
 
 
 def matches(z, c, target):
@@ -58,8 +59,7 @@
     down_hbm,
     out_ref,
     latent_ref,
-    key_w_ref,
-    value_w_ref,
+    kv_w,
     query_ref,
     query_turn_ref,
     residual_ref,
@@ -72,6 +72,8 @@
     totals,
     staged,
     heads,
+    staged_logs,
+    logs,
     hidden_ref,
     notes,
     padded,
@@ -91,6 +93,10 @@
     weight_sem,
     chunk_send,
     chunk_recv,
+    cross_send,
+    cross_recv,
+    pair_send,
+    pair_recv,
     key_send,
     key_recv,
     rot_send,
@@ -122,23 +128,29 @@
     ring = ({"sp_0": lax.rem(z + 1, ring_size)}, {"sp_0": lax.rem(z + ring_size - 1, ring_size)})
     near = ({"sp_1": 1 - c}, {"tp": mirror}, {"sp_1": 1 - c, "tp": mirror})
     others = [{"tp": lax.rem(x + r, tp)} for r in range(1, tp)]
+    groups = lax.axis_size("grp")
+    shared = groups % 2 == 0
+    parity = lax.rem(lax.axis_index("grp"), 2)
+    across = {"grp": lax.axis_index("grp") + 1 - 2 * parity}
     steps = store.shape[0]
     end = steps - 1
-    tokens = latent_ref.shape[0]
+    tokens = query_ref.shape[1]
+    half_tokens = latent_ref.shape[0]
     rows, width = residual_ref.shape
     heads_dev = query.shape[0]
-    key_width = key_w_ref.shape[1]
+    key_width = kv_w.shape[2] // 2
     span = 2 * SLOTS
+    later = x // (tp // 2)
 
     loads = [
         pltpu.make_async_copy(source, target, load_sem.at[i])
         for i, (source, target) in enumerate(
             (
-                (latent_hbm, latent_ref),
-                (key_w_hbm, key_w_ref),
-                (value_w_hbm, value_w_ref),
-                (query_turn_hbm, query_turn_ref),
-                (query_hbm, query_ref),
+                (latent_hbm.at[pl.ds(later * half_tokens, half_tokens)], latent_ref),
+                (key_w_hbm, kv_w.at[0, :, pl.ds(0, key_width)]),
+                (value_w_hbm, kv_w.at[0, :, pl.ds(key_width, key_width)]),
+                (query_turn_hbm, query_turn_ref.at[0]),
+                (query_hbm, query_ref.at[0]),
                 (residual_hbm, residual_ref),
                 (out_w_hbm, out_w),
             )
@@ -156,7 +168,7 @@
         load.start()
 
     barrier = pltpu.get_barrier_semaphore()
-    greeted = (*ring, near[0], near[2], *others)
+    greeted = (*ring, near[0], near[2], *others, *((across,) if shared else ()))
     for peer in greeted:
         pl.semaphore_signal(barrier, inc=1, device_id=peer, device_id_type=MESH)
 
@@ -170,11 +182,18 @@
             device_id_type=MESH,
         )
 
+    chunks = 3 * CHUNKS if shared else 6 * CHUNKS
+
+    def chunk_parts(i):
+        each = chunks // 3
+        kind, at = i // each, i % each
+        source, target = ((gate_hbm, gate_w), (up_hbm, up_w), (down_hbm, down_w))[kind]
+        size = source.shape[1] // (2 * CHUNKS)
+        first = parity * (CHUNKS * size) if shared else 0
+        return source, target, pl.ds(pl.multiple_of(first + at * size, size), size)
+
     def chunk_copy(i):
-        kind, at = i // CHUNKS, i % CHUNKS
-        source, target = ((gate_hbm, gate_w), (up_hbm, up_w), (down_hbm, down_w))[kind]
-        size = source.shape[1] // CHUNKS
-        part = pl.ds(at * size, size)
+        source, target, part = chunk_parts(i)
         return remote(
             source.at[0, part],
             target.at[1, part],
@@ -183,24 +202,162 @@
             {"tp": mate},
         )
 
-    issued = []
+    def cross_copy(i):
+        _, target, part = chunk_parts(i)
+        return remote(
+            target.at[1, part], target.at[1, part], cross_send.at[i], cross_recv.at[i], across
+        )
+
+    issued, crossed = [], []
 
     def issue_chunks(upto):
-        while len(issued) < min(upto, 3 * CHUNKS):
+        while len(issued) < min(upto, chunks):
             chunk_copy(len(issued)).start()
             issued.append(None)
 
-    def active(d, j, h):
-        return j < end or h * 2 // SPLIT == d
-
-    for j in range(steps):
+    def cross_chunks(upto):
+        while shared and len(crossed) < min(upto, chunks):
+            chunk_copy(len(crossed)).wait_recv()
+            cross_copy(len(crossed)).start()
+            crossed.append(None)
+
+    def active(d, j, h, split):
+        return j < end or h * 2 // split == d
+
+    loads[0].wait()
+    wide = latent_ref[...].astype(jnp.float32)
+    mine = slice(half_tokens, 2 * half_tokens)
+    store[end, mine] = (
+        wide
+        * lax.rsqrt(jnp.mean(wide * wide, axis=-1, keepdims=True) + eps)
+        * gain_ref[...].astype(jnp.float32)
+    ).astype(jnp.bfloat16)
+    for load in loads[1:5]:
+        load.wait()
+    pl.semaphore_wait(barrier, len(greeted))
+
+    latent_part = store.shape[2] // KEY_SPLIT
+    depth = kv_w.shape[1] // 2
+
+    def key_copy(d, j, h):
+        source_step, source_slot = (end, 1) if j == 0 else (j - 1, d)
+        slot = d if j < end else 0
+        columns = pl.ds(h * latent_part, latent_part)
+        return remote(
+            store.at[source_step, pl.ds(source_slot * half_tokens, half_tokens), columns],
+            store.at[j, pl.ds(slot * half_tokens, half_tokens), columns],
+            key_send.at[d, j, h],
+            key_recv.at[d, j, h],
+            ring[d],
+        )
+
+    def rot_copy(d, j):
+        return remote(
+            rots.at[end, 1] if j == 0 else rots.at[j - 1, d],
+            rots.at[j, d],
+            rot_send.at[d, j],
+            rot_recv.at[d, j],
+            ring[d],
+        )
+
+    def note_copy(d, j):
+        return remote(
+            notes.at[1, end] if j == 0 else notes.at[d, j - 1],
+            notes.at[d, j],
+            note_send.at[d, j],
+            note_recv.at[d, j],
+            ring[d],
+        )
+
+    def side_copy(d, j):
+        return remote(
+            store.at[j, pl.ds(d * half_tokens, half_tokens)],
+            store.at[j, pl.ds((2 + d) * half_tokens, half_tokens)],
+            side_send.at[d, j],
+            side_recv.at[d, j],
+            near[0],
+        )
+
+    def side_rot_copy(d, j):
+        return remote(
+            rots.at[j, d],
+            rots.at[j, 2 + d],
+            side_rot_send.at[d, j],
+            side_rot_recv.at[d, j],
+            near[0],
+        )
+
+    core_rows = pl.ds(pl.multiple_of(c * depth, depth), depth)
+    pair_copies = [
+        remote(source, target, pair_send.at[i], pair_recv.at[i], near[1])
+        for i, (source, target) in enumerate(
+            (
+                (query_turn_ref.at[0], query_turn_ref.at[1]),
+                (query_ref.at[0], query_ref.at[1]),
+                (kv_w.at[0, core_rows], kv_w.at[1, core_rows]),
+            )
+        )
+    ]
+    other_rows = pl.ds(pl.multiple_of((1 - c) * depth, depth), depth)
+    pair_side = remote(
+        kv_w.at[1, core_rows], kv_w.at[1, core_rows], pair_send.at[3], pair_recv.at[3], near[0]
+    )
+
+    def tp_copy(r, kind):
+        source, target = ((staged, heads), (staged_logs, logs))[kind]
+        return remote(
+            source.at[lax.rem(x + r, tp)],
+            target.at[x],
+            tp_send.at[r - 1, kind],
+            tp_recv.at[r - 1, kind],
+            others[r - 1],
+        )
+
+    log2e = 1.4426950408889634
+    factor = (PLAIN_HEAD_WIDTH + QK_ROPE) ** (-0.5) * log2e
+
+    def attend(j, side):
+        if side:
+            for d in range(2):
+                side_copy(d, j).wait_recv()
+                side_rot_copy(d, j).wait_recv()
+        at = slice(2 * side * half_tokens, 2 * (side + 1) * half_tokens)
+        latents = store[j, at]
+        spins = rots[j, 2 * side : 2 * side + 2].reshape(2 * half_tokens, 2 * QK_ROPE)
+        for owner in range(2):
+            both = jnp.dot(latents, kv_w[owner], preferred_element_type=jnp.float32).astype(
+                jnp.bfloat16
+            )
+            for local in range(heads_dev // 2):
+                head = owner * (heads_dev // 2) + local
+                first = local * PLAIN_HEAD_WIDTH
+                keys = jnp.concatenate([both[:, first : first + PLAIN_HEAD_WIDTH], spins], axis=1)
+                scores = lax.dot_general(
+                    query[head],
+                    keys,
+                    (((1,), (1,)), ((), ())),
+                    preferred_element_type=jnp.float32,
+                )
+                before = peaks[head]
+                peak = jnp.maximum(before, jnp.max(scores, axis=1, keepdims=True))
+                weights = jnp.exp2((scores - peak[:, 0:1]) * factor)
+                keep = jnp.exp2((before - peak) * factor)
+                totals[head] = totals[head] * keep + jnp.sum(weights, axis=1, keepdims=True)
+                first = key_width + local * VALUE_WIDTH
+                summed[head] = summed[head] * keep + jnp.dot(
+                    weights.astype(jnp.bfloat16),
+                    both[:, first : first + VALUE_WIDTH],
+                    preferred_element_type=jnp.float32,
+                )
+                peaks[head] = peak
+
+    for h in range(KEY_SPLIT):
         for d in range(2):
-            blocks[j, d * HALF + rows : (d + 1) * HALF] = jnp.zeros(
-                (HALF - rows, width), blocks.dtype
-            )
-    summed[...] = jnp.zeros_like(summed)
-    totals[...] = jnp.zeros_like(totals)
-    peaks[...] = jnp.full_like(peaks, -jnp.inf)
+            key_copy(d, 0, h).start()
+    side_copy(1, end).start()
+    for copy in pair_copies:
+        copy.start()
+    issue_chunks(3)
 
     lane = lax.broadcasted_iota(jnp.int32, (tokens, 2 * QK_ROPE), 1)
     place = lax.broadcasted_iota(jnp.int32, (tokens, 2 * QK_ROPE), 0) + (2 * z + c) * tokens
@@ -223,10 +380,12 @@
     flat = jnp.transpose(key_turn_ref[...].astype(jnp.float32))
     twice = turned(jnp.concatenate([flat, flat], axis=1))
     left = lane < QK_ROPE
-    rots[end, 2] = jnp.where(
-        left[: tokens // 2], twice[: tokens // 2], twice[tokens // 2 :]
-    ).astype(jnp.bfloat16)
-
+    rots[end, 1] = jnp.where(later == 0, twice[:half_tokens], twice[half_tokens:]).astype(
+        jnp.bfloat16
+    )
+    for d in range(2):
+        rot_copy(d, 0).start()
+    side_rot_copy(1, end).start()
     padded[0] = jnp.full(padded.shape[1:], -1.0, jnp.float32)
     padded[1] = jnp.zeros(padded.shape[1:], jnp.float32)
     top = routes_ref.shape[0]
@@ -251,172 +410,106 @@
         notes[1, end, k : k + 1] = padded[0, k : k + 1] * SLOTS + slot
         notes[1, end, top + k : top + k + 1] = padded[1, k : k + 1]
 
-    for load in loads[:3]:
-        load.wait()
-    wide = latent_ref[...].astype(jnp.float32)
-    wide = (
-        wide
-        * lax.rsqrt(jnp.mean(wide * wide, axis=-1, keepdims=True) + eps)
-        * gain_ref[...].astype(jnp.float32)
-    ).astype(jnp.bfloat16)
-    mine = slice(2 * tokens, 3 * tokens)
-    store[end, mine, 0:key_width] = jnp.dot(
-        wide, key_w_ref[...], preferred_element_type=jnp.float32
-    ).astype(jnp.bfloat16)
-    store[end, mine, key_width:] = jnp.dot(
-        wide, value_w_ref[...], preferred_element_type=jnp.float32
-    ).astype(jnp.bfloat16)
-    pl.semaphore_wait(barrier, len(greeted))
-
-    piece = tokens // SPLIT
-
-    def key_copy(d, j, h):
-        source_step, source_slot = (end, 2) if j == 0 else (j - 1, 2 * d)
-        slot = 2 * d if j < end else 0
-        return remote(
-            store.at[source_step, pl.ds(source_slot * tokens + h * piece, piece)],
-            store.at[j, pl.ds(slot * tokens + h * piece, piece)],
-            key_send.at[d, j, h],
-            key_recv.at[d, j, h],
-            ring[d],
-        )
-
-    def rot_copy(d, j):
-        return remote(
-            rots.at[end, 2] if j == 0 else rots.at[j - 1, 2 * d],
-            rots.at[j, 2 * d],
-            rot_send.at[d, j],
-            rot_recv.at[d, j],
-            ring[d],
-        )
-
-    def note_copy(d, j):
-        return remote(
-            notes.at[1, end] if j == 0 else notes.at[d, j - 1],
-            notes.at[d, j],
-            note_send.at[d, j],
-            note_recv.at[d, j],
-            ring[d],
-        )
-
-    def side_copy(d, j):
-        return remote(
-            store.at[j, pl.ds(2 * d * tokens, tokens)],
-            store.at[j, pl.ds((2 * d + 1) * tokens, tokens)],
-            side_send.at[d, j],
-            side_recv.at[d, j],
-            near[0],
-        )
-
-    def side_rot_copy(d, j):
-        return remote(
-            rots.at[j, 2 * d],
-            rots.at[j, 2 * d + 1],
-            side_rot_send.at[d, j],
-            side_rot_recv.at[d, j],
-            near[0],
-        )
-
-    def tp_copy(r):
-        return remote(
-            staged.at[lax.rem(x + r, tp)],
-            heads.at[x],
-            tp_send.at[r - 1],
-            tp_recv.at[r - 1],
-            others[r - 1],
-        )
-
-    factor = (PLAIN_HEAD_WIDTH + QK_ROPE) ** (-0.5) * 1.4426950408889634
-
-    def attend(j):
-        for d in range(2):
-            side_copy(d, j).wait_recv()
-            side_rot_copy(d, j).wait_recv()
-        pairs = []
-        for b in range(4):
-            pair = rots[j, b]
-            pairs.append(pair)
-            pairs.append(jnp.concatenate([pair[:, QK_ROPE:], pair[:, :QK_ROPE]], axis=1))
-        pairs = jnp.concatenate(pairs, axis=0)
-        for head in range(heads_dev):
-            at = head * PLAIN_HEAD_WIDTH
-            keys = jnp.concatenate([store[j, :, at : at + PLAIN_HEAD_WIDTH], pairs], axis=1)
-            scores = lax.dot_general(
-                query[head],
-                keys,
-                (((1,), (1,)), ((), ())),
-                preferred_element_type=jnp.float32,
-            )
-            before = peaks[head]
-            peak = jnp.maximum(before, jnp.max(scores, axis=1, keepdims=True))
-            weights = jnp.exp2((scores - peak[:, 0:1]) * factor)
-            keep = jnp.exp2((before - peak) * factor)
-            totals[head] = totals[head] * keep + jnp.sum(weights, axis=1, keepdims=True)
-            at = key_width + head * VALUE_WIDTH
-            summed[head] = summed[head] * keep + jnp.dot(
-                weights.astype(jnp.bfloat16),
-                store[j, :, at : at + VALUE_WIDTH],
-                preferred_element_type=jnp.float32,
-            )
-            peaks[head] = peak
-
-    for h in range(SPLIT):
-        for d in range(2):
-            key_copy(d, 0, h).start()
-            if h == 0:
-                rot_copy(d, 0).start()
-    side_copy(1, end).start()
-    side_rot_copy(1, end).start()
     for d in range(2):
         note_copy(d, 0).start()
-    issue_chunks(2)
-    for load in loads[3:5]:
-        load.wait()
-    spun = turned(query_turn_ref[...].astype(jnp.float32))
-    for head in range(heads_dev):
-        query[head, :, 0:PLAIN_HEAD_WIDTH] = query_ref[
-            :, head * PLAIN_HEAD_WIDTH : (head + 1) * PLAIN_HEAD_WIDTH
-        ]
-        here = spun if head == 0 else pltpu.roll(spun, 2 * QK_ROPE - head * QK_ROPE, 1)
-        query[head, :, PLAIN_HEAD_WIDTH:] = jnp.where(left, here, 0.0).astype(jnp.bfloat16)
+    summed[...] = jnp.zeros_like(summed)
+    totals[...] = jnp.zeros_like(totals)
+    peaks[...] = jnp.full_like(peaks, -jnp.inf)
+
+    def place_queries(owner):
+        spun = turned(query_turn_ref[owner].astype(jnp.float32))
+        for local in range(heads_dev // 2):
+            head = owner * (heads_dev // 2) + local
+            query[head, :, 0:PLAIN_HEAD_WIDTH] = query_ref[
+                owner, :, local * PLAIN_HEAD_WIDTH : (local + 1) * PLAIN_HEAD_WIDTH
+            ]
+            here = spun if local == 0 else pltpu.roll(spun, 2 * QK_ROPE - local * QK_ROPE, 1)
+            query[head, :, PLAIN_HEAD_WIDTH:] = jnp.where(left, here, 0.0).astype(jnp.bfloat16)
+
+    place_queries(0)
+    plan = [[] for _ in range(steps)]
+    plan[1] = [(0, 0), (0, 1)]
+    plan[2] = [(1, 0), (1, 1), (2, 0)]
+    for j in range(3, steps):
+        plan[j] = [(j - 1, 1), (j, 0)]
     for j in range(steps):
-        for h in range(SPLIT):
+        for h in range(KEY_SPLIT):
             for d in range(2):
-                if active(d, j, h):
+                if active(d, j, h, KEY_SPLIT):
                     key_copy(d, j, h).wait_recv()
-                    if j < end and active(d, j + 1, h):
+                    if j < end and active(d, j + 1, h, KEY_SPLIT):
                         key_copy(d, j + 1, h).start()
-                if h == 0 and j <= end - d:
-                    rot_copy(d, j).wait_recv()
-                    if j < end - d:
-                        rot_copy(d, j + 1).start()
         for d in range(2):
             if j <= end - d:
                 side_copy(d, j).start()
+                rot_copy(d, j).wait_recv()
+                if j < end - d:
+                    rot_copy(d, j + 1).start()
                 side_rot_copy(d, j).start()
                 note_copy(d, j).wait_recv()
                 if j < end - d:
                     note_copy(d, j + 1).start()
         if j < end:
-            issue_chunks(2 + (j + 1) * 3 // 2)
-        if j > 0:
-            attend(j - 1)
-    attend(end)
-    done = jnp.concatenate([summed[head] / totals[head] for head in range(heads_dev)], axis=1)
+            issue_chunks(4 + j)
+        if j == 0:
+            for p in range(steps):
+                for d in range(2):
+                    blocks[p, d * HALF + rows : (d + 1) * HALF] = jnp.zeros(
+                        (HALF - rows, width), blocks.dtype
+                    )
+        if j == 1:
+            pair_copies[2].wait_recv()
+            pair_side.start()
+            for copy in pair_copies[:2]:
+                copy.wait_recv()
+            place_queries(1)
+            pair_side_in = remote(
+                kv_w.at[1, other_rows], kv_w.at[1, other_rows], pair_send.at[3], pair_recv.at[3], near[0]
+            )
+            pair_side_in.wait_recv()
+        for unit in plan[j]:
+            attend(*unit)
+        cross_chunks(j - 1)
+    attend(end, 1)
+    logs_all = jnp.zeros((tokens, 2 * QK_ROPE), jnp.float32)
+    done = []
+    for head in range(heads_dev):
+        total = totals[head]
+        done.append(summed[head] / total)
+        logs_all = jnp.where(
+            lane == head, peaks[head] * factor + jnp.log(total) * log2e, logs_all
+        )
+    done = jnp.concatenate(done, axis=1)
     for t in range(tp):
         staged[t] = done[t * rows : (t + 1) * rows].astype(jnp.bfloat16)
+        staged_logs[t] = logs_all[t * rows : (t + 1) * rows]
     for r in range(1, tp):
-        tp_copy(r).start()
+        for kind in range(2):
+            tp_copy(r, kind).start()
     heads[x] = staged[x]
+    logs[x] = staged_logs[x]
     for load in loads[5:]:
         load.wait()
     for r in range(1, tp):
-        tp_copy(r).wait_recv()
+        for kind in range(2):
+            tp_copy(r, kind).wait_recv()
     total = residual_ref[...].astype(jnp.float32)
-    head_width = heads.shape[2]
     for t in range(tp):
+        joined = []
+        for local in range(heads_dev // 2):
+            alone = []
+            for owner, source in enumerate((t, tp - 1 - t)):
+                head = owner * (heads_dev // 2) + local
+                part = heads[source, :, head * VALUE_WIDTH : (head + 1) * VALUE_WIDTH]
+                alone.append((part.astype(jnp.float32), logs[source][:, head : head + 1]))
+            (a, log_a), (b, log_b) = alone
+            top_log = jnp.maximum(log_a, log_b)
+            share_a, share_b = jnp.exp2(log_a - top_log), jnp.exp2(log_b - top_log)
+            joined.append((a * share_a + b * share_b) / (share_a + share_b))
+        joined = jnp.concatenate(joined, axis=1).astype(jnp.bfloat16)
+        head_width = joined.shape[1]
         total = total + jnp.dot(
-            heads[t],
+            joined,
             out_w[t * head_width : (t + 1) * head_width],
             preferred_element_type=jnp.float32,
         )
@@ -429,7 +522,7 @@
         * ffn_gain_ref[...].astype(jnp.float32)
     ).astype(jnp.bfloat16)
 
-    part = width // SPLIT
+    part = width // ROW_SPLIT
 
     def row_copy(d, j, h):
         columns = pl.ds(h * part, part)
@@ -474,16 +567,16 @@
     def merged(j):
         return jnp.concatenate([notes[0, j][:, :HALF], notes[1, j][:, :HALF]], axis=1)
 
-    for h in range(SPLIT):
+    for h in range(ROW_SPLIT):
         for d in range(2):
             row_copy(d, 0, h).start()
-    issue_chunks(15)
+    issue_chunks(chunks if shared else chunks // 2)
     for j in range(steps):
-        for h in range(SPLIT):
+        for h in range(ROW_SPLIT):
             for d in range(2):
-                if active(d, j, h):
+                if active(d, j, h, ROW_SPLIT):
                     row_copy(d, j, h).wait_recv()
-                    if j < end and active(d, j + 1, h):
+                    if j < end and active(d, j + 1, h, ROW_SPLIT):
                         row_copy(d, j + 1, h).start()
         picks = sum(m.astype(jnp.float32) for m in matches(z, c, merged(j))).astype(jnp.bfloat16)
         kept = jnp.dot(picks, blocks[j], preferred_element_type=jnp.float32).astype(jnp.bfloat16)
@@ -491,8 +584,10 @@
         for q in (2, 3, 1):
             go_copy(j, q).start()
         taken[j, 0:span] = kept[0:span]
-        issue_chunks(15 + (j + 1) * 3 // 2)
-    issue_chunks(3 * CHUNKS)
+        issue_chunks(chunks // 2 + 2 * (j + 1))
+        cross_chunks(end - 1 + j)
+    issue_chunks(chunks)
+    cross_chunks(chunks)
 
     group = steps // 2
     for i, (a, b) in enumerate(((group, steps), (0, group))):
@@ -506,8 +601,8 @@
                 if i == 0 and half == 0:
                     own_weights[kind].wait()
                 elif i == 0:
-                    for at in range(CHUNKS):
-                        chunk_copy(kind * CHUNKS + at).wait_recv()
+                    for at in range(kind * chunks // 3, (kind + 1) * chunks // 3):
+                        (cross_copy if shared else chunk_copy)(at).wait_recv()
 
             ready(0)
             gate = jnp.minimum(
@@ -545,19 +640,19 @@
         )
         if j == end:
             own_part[...] = token[HALF : HALF + rows]
-        for h in range(SPLIT):
+        for h in range(ROW_SPLIT):
             columns = slice(h * part, (h + 1) * part)
             for d in range(2):
-                if not active(d, j, h):
+                if not active(d, j, h, ROW_SPLIT):
                     continue
                 at = d * HALF if j < end else 0
                 total = token[at : at + rows, columns]
-                if j < end and active(d, j + 1, h):
+                if j < end and active(d, j + 1, h, ROW_SPLIT):
                     sum_copy(d, j + 1, h).wait_recv()
                     total = total + arrive[d, j, :, columns].astype(jnp.float32)
                 leave[d, j, :, columns] = total.astype(jnp.bfloat16)
                 sum_copy(d, j, h).start()
-    for h in range(SPLIT):
+    for h in range(ROW_SPLIT):
         columns = slice(h * part, (h + 1) * part)
         for d in range(2):
             sum_copy(d, 0, h).wait_recv()
@@ -568,15 +663,22 @@
             + arrive[1, end, :, columns].astype(jnp.float32)
         ).astype(jnp.bfloat16)
 
-    for i in range(3 * CHUNKS):
+    for i in range(chunks):
         chunk_copy(i).wait_send()
+        if shared:
+            cross_copy(i).wait_send()
+    for copy in (*pair_copies, pair_side):
+        copy.wait_send()
     for r in range(1, tp):
-        tp_copy(r).wait_send()
+        for kind in range(2):
+            tp_copy(r, kind).wait_send()
     for j in range(steps):
         for d in range(2):
-            for h in range(SPLIT):
-                if active(d, j, h):
+            for h in range(KEY_SPLIT):
+                if active(d, j, h, KEY_SPLIT):
                     key_copy(d, j, h).wait_send()
+            for h in range(ROW_SPLIT):
+                if active(d, j, h, ROW_SPLIT):
                     row_copy(d, j, h).wait_send()
                     sum_copy(d, j, h).wait_send()
             if j <= end - d:
@@ -606,9 +708,10 @@
     routes,
     route_weights,
 ):
-    tokens = latent.shape[0]
+    tokens, latent_width = latent.shape
+    half_tokens = tokens // 2
     rows, width = residual.shape
-    heads_dev = query_plain.shape[1] // PLAIN_HEAD_WIDTH
+    heads_dev = 2 * query_plain.shape[1] // PLAIN_HEAD_WIDTH
     tp = lax.axis_size("tp")
     steps = lax.axis_size("sp_0") // 2
     store_width = plain_key_matrix.shape[1] + value_matrix.shape[1]
@@ -635,7 +738,7 @@
         (down_weight, anywhere),
     )
     both_ways = dma((2, steps))
-    pieces = dma((2, steps, SPLIT))
+    pieces = dma((2, steps, ROW_SPLIT))
     return pl.pallas_call(
         layer_kernel,
         name="layer",
@@ -643,21 +746,22 @@
         in_specs=[pl.BlockSpec(memory_space=space) for _, space in operands],
         out_specs=pl.BlockSpec(memory_space=vmem),
         scratch_shapes=[
-            vmem(latent.shape, bf16),
-            vmem(plain_key_matrix.shape, bf16),
-            vmem(value_matrix.shape, bf16),
-            vmem(query_plain.shape, bf16),
-            vmem(query_turn.shape, bf16),
+            vmem((half_tokens, latent_width), bf16),
+            vmem((2, latent_width, store_width), bf16),
+            vmem((2, *query_plain.shape), bf16),
+            vmem((2, *query_turn.shape), bf16),
             vmem(residual.shape, bf16),
             vmem(out_weight.shape, bf16),
             vmem((heads_dev, tokens, PLAIN_HEAD_WIDTH + 2 * QK_ROPE), bf16),
-            vmem((steps, 4 * tokens, store_width), bf16),
-            vmem((steps, 4, tokens // 2, 2 * QK_ROPE), bf16),
+            vmem((steps, 4 * half_tokens, latent_width), bf16),
+            vmem((steps, 4, half_tokens, 2 * QK_ROPE), bf16),
             vmem((heads_dev, tokens, VALUE_WIDTH), f32),
             vmem((heads_dev, tokens, VALUE_WIDTH), f32),
             vmem((heads_dev, tokens, VALUE_WIDTH), f32),
             vmem((tp, rows, head_width), bf16),
             vmem((tp, rows, head_width), bf16),
+            vmem((tp, rows, 2 * QK_ROPE), f32),
+            vmem((tp, rows, 2 * QK_ROPE), f32),
             vmem((rows, width), bf16),
             vmem((2, steps, 8, 2 * HALF), f32),
             vmem((2, 8, 2 * HALF), f32),
@@ -675,10 +779,14 @@
             vmem((2, steps, rows, width), bf16),
             dma((7,)),
             dma((3,)),
+            dma((6 * CHUNKS,)),
+            dma((6 * CHUNKS,)),
             dma((3 * CHUNKS,)),
             dma((3 * CHUNKS,)),
-            pieces,
-            pieces,
+            dma((4,)),
+            dma((4,)),
+            dma((2, steps, KEY_SPLIT)),
+            dma((2, steps, KEY_SPLIT)),
             both_ways,
             both_ways,
             both_ways,
@@ -687,8 +795,8 @@
             both_ways,
             both_ways,
             both_ways,
-            dma((tp - 1,)),
-            dma((tp - 1,)),
+            dma((tp - 1, 2)),
+            dma((tp - 1, 2)),
             pieces,
             pieces,
             dma((steps, 3)),

time: 161 us -> 154 us (0.957)
  Pallas kernels: 156 us -> 149 us
    pallas_call x1, Pallas kernels: 156 us -> 149 us  [on_device(): pl.pallas_call(layer_kernel, name='layer', out_shape=jax.ShapeDtypeStruct...]
where the time goes in v4:
time: 154 us; the launch traced here: 153 us
  Pallas kernels  149 us (97%)
  local copies, waits for them, and re-layouts  4.12 us (3%)
    pallas_call x1, Pallas kernels, on_device(): pl.pallas_call(layer_kernel, name='layer', out_shape=jax.ShapeDtypeStruct...  149 us

profile of v4, /device:TPU:40, one launch (start us, length us, event | category | flops | bytes accessed | tf_op | source)
XLA Modules:
  0.0 153.4 jit_solution(13793192451221658940)
XLA Ops:
  0.0 1.2 reshape.6.gain_ref
  1.2 1.3 reshape.7.ffn_gain_ref
  2.5 149.3 %layer.1 = bf16[40,2048]{1,0:T(8,128)(2,1)} custom-call(bf16[160,512]{1,0:T(8,128)(2,1)} %latent_hbm.1, bf16[1,512]{1,0:T(2,128)(2,1)} %reshape.6.gain_ref, bf16[512,256]{1,0:T(8,128)(2,1)} %key_w_hbm.1, bf16[512,256]{1,0:T(8,128)(2,1)} %value_w_hbm.1, bf16[64,160]{1,0:T(8,128)(2,1)} %bitcast.3, bf16[160,256]{1,0:T(8,128)(2,1)} %query_hbm.1, ...), custom_call_target="tpu_custom_call" | custom-call | flops 30000001024 | bytes 20000000 | tf_op jit(solution)/shard_map/layer/pallas_call | solution.py:742
  151.8 1.6 %copy.17 = bf16[40,2048]{1,0:T(8,128)(2,1)} copy(bf16[40,2048]{1,0:T(8,128)(2,1)} %layer.1) | data formatting | bytes 327680
